TPU v7x, 256 devices: a whole 4x4x8 slice. The times are simulated.
256 devices in a mesh: ep: 16 (over y, x), tp: 16 (over z, core).
Axes of the slice: x: 4, y: 4, z: 8, core: 2. Of those that a mesh axis runs over, the one named last changes fastest.
Arguments:
- tokens: bfloat16 [1024, 2048], P('ep', 'tp'), may hold values from -6 to 6
- prior_state: float32 [1024, 16, 64, 128], P('ep', 'tp'), may hold values from -3 to 3
- decay_rate: float32 [16], P('tp'), may hold values from 0.01 to 0.5
- norm_in: float32 [2048], replicated, may hold values from 0.1 to 1.9
- query_weight: bfloat16 [2048, 1024], P(None, 'tp'), may hold values from -0.125 to 0.125
- key_weight: bfloat16 [2048, 1024], P(None, 'tp'), may hold values from -0.125 to 0.125
- value_weight: bfloat16 [2048, 2048], P(None, 'tp'), may hold values from -0.125 to 0.125
- gate_weight: bfloat16 [2048, 2048], P(None, 'tp'), may hold values from -0.125 to 0.125
- out_weight: bfloat16 [2048, 2048], P('tp'), may hold values from -0.125 to 0.125
- norm_moe: float32 [2048], replicated, may hold values from 0.1 to 1.9
- routes: int32 [1024, 2], replicated, may hold values from 0 to 15, all different within a row; in each aligned block of 64 rows (0 to 63, 64 to 127, ...) at most 12 rows name the same one
- route_weight: float32 [1024, 2], replicated, may hold values from 0.1 to 1
- expert_gate: bfloat16 [16, 2048, 7168], P('ep', None, 'tp'), may hold values from -0.125 to 0.125
- expert_up: bfloat16 [16, 2048, 7168], P('ep', None, 'tp'), may hold values from -0.125 to 0.125
- expert_down: bfloat16 [16, 7168, 2048], P('ep', 'tp'), may hold values from -0.0625 to 0.0625
Outputs:
- next_hidden: bfloat16 [1024, 2048], P('ep', 'tp')
- new_state: float32 [1024, 16, 64, 128], P('ep', 'tp')
Inputs may be any that keep to these rules, and one draw needn't show every extreme that they name: `routes`: the 2 experts of a row differ. In each aligned block of 64 rows (the sequences of one index of ep), no expert is named by more than 12 rows, a bound that some block reaches.
All inputs are finite; a program needn't handle non-finite values.
Results may differ from a plain program's by a relative error of at most 0.011.
Values may be sent and summed in bfloat16 or wider, within the bound.
A program may use at most 64 MiB of HBM per device.

v0:
```python
import jax
import jax.numpy as jnp
from jax import lax
from jax.sharding import PartitionSpec as P

DK = 64
DV = 128


EPSILON = 1e-06


def in_order(blocks, dim):
    blocks = jnp.moveaxis(blocks, 0, dim)
    dims = blocks.shape
    return blocks.reshape(*dims[:dim], dims[dim] * dims[dim + 1], *dims[dim + 2 :])


def sent_to_all(array, axis):
    copies = jnp.broadcast_to(array, (lax.axis_size(axis), *array.shape))
    return lax.all_to_all(copies, axis, split_axis=0, concat_axis=0, tiled=True)


def gather_directly(array, axis, dim):
    return in_order(sent_to_all(array, axis), dim)


def split_up(array, dim, peers):
    before, after = (array.shape[:dim], array.shape[dim + 1 :])
    return jnp.moveaxis(array.reshape(*before, peers, -1, *after), dim, 0)


def sum_at_owner(array, axis, dim):
    blocks = split_up(array, dim, lax.axis_size(axis))
    arrived = lax.all_to_all(blocks, axis, split_axis=0, concat_axis=0, tiled=True)
    return arrived.astype(jnp.float32).sum(axis=0)


def rms_scale(row_block, gain_row):
    values = row_block.astype(jnp.float32)
    factor = lax.rsqrt(jnp.mean(values * values, -1, keepdims=True) + EPSILON)
    return (values * factor * gain_row).astype(jnp.bfloat16)


def project(normed_in, weight):
    stored = jnp.dot(normed_in, weight, preferred_element_type=jnp.float32).astype(jnp.bfloat16)
    return lax.optimization_barrier(stored).astype(jnp.float32)


def route_tables(route_rows, weight_rows, expert_count):
    labels = jnp.arange(expert_count, dtype=jnp.int32)
    match = route_rows[:, :, None] == labels[None, None, :]
    chosen = jnp.sum(match.astype(jnp.int32), 1)
    weighted = jnp.sum(jnp.where(match, weight_rows[:, :, None], 0.0), 1)
    return (chosen, weighted)


def slot_table(chosen, capacity):
    rank = jnp.cumsum(chosen, 0) - chosen
    slot_ids = jnp.arange(capacity, dtype=jnp.int32)
    return (rank[:, :, None] == slot_ids[None, None, :]) & (chosen[:, :, None] > 0)


def on_device(
    tokens,
    prior_state,
    decay_rate,
    norm_in,
    query_weight,
    key_weight,
    value_weight,
    gate_weight,
    out_weight,
    norm_moe,
    routes,
    route_weight,
    expert_gate,
    expert_up,
    expert_down,
):
    row_count = tokens.shape[0]
    own_width = tokens.shape[1]
    head_count = prior_state.shape[1]
    full_tokens = gather_directly(tokens, "tp", 1)
    full_width = full_tokens.shape[1]
    normed_in = rms_scale(full_tokens, norm_in)
    query = project(normed_in, query_weight).reshape(row_count, head_count, DK)
    keyed = project(normed_in, key_weight).reshape(row_count, head_count, DK) * DK ** (-0.5)
    valued = project(normed_in, value_weight).reshape(row_count, head_count, DV)
    gate_pre = project(normed_in, gate_weight)
    keep = (1.0 - decay_rate)[None, :, None, None]
    new_state = keep * prior_state + jnp.einsum(
        "bhk,bhv->bhkv", keyed, valued, precision=lax.Precision.HIGHEST
    )
    read = jnp.einsum("bhk,bhkv->bhv", query, new_state, precision=lax.Precision.HIGHEST)
    centred = read - jnp.mean(read, -1, keepdims=True)
    normed = centred * lax.rsqrt(jnp.mean(centred * centred, -1, keepdims=True) + EPSILON)
    mixed_heads = (jax.nn.silu(gate_pre) * normed.reshape(row_count, head_count * DV)).astype(
        jnp.bfloat16
    )
    partial_value = jnp.dot(mixed_heads, out_weight, preferred_element_type=jnp.float32)
    mixer_part = sum_at_owner(partial_value.astype(jnp.bfloat16), "tp", 1)
    resid_own = (tokens.astype(jnp.float32) + mixer_part).astype(jnp.bfloat16)
    resid_rows = gather_directly(resid_own, "tp", 1)
    expert_in = rms_scale(resid_rows, norm_moe)
    groups = lax.axis_size("ep")
    local_experts = expert_gate.shape[0]
    experts_all = local_experts * groups
    top_count = routes.shape[1]
    capacity = (3 * top_count * row_count + 2 * experts_all - 1) // (2 * experts_all)
    start = lax.axis_index("ep") * row_count
    own_routes = lax.dynamic_slice_in_dim(routes, start, row_count, 0)
    own_weights = lax.dynamic_slice_in_dim(route_weight, start, row_count, 0)
    chosen, weighted = route_tables(own_routes, own_weights, experts_all)
    hit = slot_table(chosen, capacity)
    place = hit.reshape(row_count, experts_all * capacity).astype(jnp.bfloat16)
    spread = jnp.where(hit, weighted[:, :, None], 0.0).reshape(row_count, experts_all * capacity)
    sent = jnp.einsum("bs,bd->sd", place, expert_in, preferred_element_type=jnp.float32)
    sent = sent.astype(jnp.bfloat16).reshape(groups, local_experts, capacity, full_width)
    received = lax.all_to_all(sent, "ep", split_axis=0, concat_axis=0, tiled=True)
    gate_part = jnp.einsum(
        "secd,edf->secf", received, expert_gate, preferred_element_type=jnp.float32
    )
    up_part = jnp.einsum("secd,edf->secf", received, expert_up, preferred_element_type=jnp.float32)
    hidden = (jax.nn.silu(gate_part) * up_part).astype(jnp.bfloat16)
    down = jnp.einsum("secf,efd->secd", hidden, expert_down, preferred_element_type=jnp.float32)
    reduced = sum_at_owner(down.astype(jnp.bfloat16), "tp", 3)
    returned = lax.all_to_all(reduced, "ep", split_axis=0, concat_axis=0, tiled=True)
    returned = returned.reshape(experts_all * capacity, own_width)
    moe_part = jnp.dot(spread, returned, precision=lax.Precision.HIGHEST)
    next_hidden = (resid_own.astype(jnp.float32) + moe_part).astype(jnp.bfloat16)
    return (next_hidden, new_state)


def solution(mesh):
    placed = (
        P("ep", "tp"),
        P("ep", "tp", None, None),
        P("tp"),
        P(),
        P(None, "tp"),
        P(None, "tp"),
        P(None, "tp"),
        P(None, "tp"),
        P("tp", None),
        P(),
        P(),
        P(),
        P("ep", None, "tp"),
        P("ep", None, "tp"),
        P("ep", "tp", None),
    )
    return jax.shard_map(
        on_device,
        mesh=mesh,
        in_specs=placed,
        out_specs=(P("ep", "tp"), P("ep", "tp", None, None)),
        check_vma=False,
    )
```

profile of v0, /device:TPU:1, one launch (start us, length us, event | category | flops | bytes accessed | tf_op | source)
XLA Modules:
  0.0 134.2 jit_solution(5371043922793690754)
XLA Ops:
  0.7 1.6 %broadcast_in_dim.24 = bf16[16,64,128]{2,1,0:T(8,128)(2,1)} broadcast(bf16[64,128]{1,0:T(8,128)(2,1)} %param.15), dimensions={1,2} | broadcast | bytes 278528 | tf_op jit(solution)/shard_map/broadcast_in_dim | solution.py:20
  2.3 10.0 %all-to-all-start = ((bf16[16,64,128]{2,1,0:T(8,128)(2,1)}), bf16[16,64,128]{2,1,0:T(8,128)(2,1)S(1)}, u32[]{:S(2)}, u32[]{:S(2)}) async-start(bf16[16,64,128]{2,1,0:T(8,128)(2,1)} %broadcast_in_dim.24), calls=%async_computation | async-start | bytes 524288 | tf_op jit(solution)/shard_map/all_to_all | solution.py:21
  12.9 10.9 %all-to-all-done = bf16[16,64,128]{2,1,0:T(8,128)(2,1)S(1)} async-done(((bf16[16,64,128]{2,1,0:T(8,128)(2,1)}), bf16[16,64,128]{2,1,0:T(8,128)(2,1)S(1)}, u32[]{:S(2)}, u32[]{:S(2)}) %all-to-all-start) | async-done | bytes 262176 | tf_op jit(solution)/shard_map/all_to_all | solution.py:21
  24.0 1.0 fusion.41
  25.0 1.3 convolution_convert_fusion.3
  27.5 1.3 copy-done.1
  28.8 1.1 fusion
  30.7 0.8 copy.74
  31.5 3.4 %all-to-all-start.1 = ((bf16[16,64,128]{2,1,0:T(8,128)(2,1)}), bf16[16,64,128]{2,1,0:T(8,128)(2,1)S(1)}, u32[]{:S(2)}, u32[]{:S(2)}) async-start(bf16[16,64,128]{2,1,0:T(8,128)(2,1)} %bitcast.124), calls=%async_computation.1 | async-start | bytes 524288 | tf_op jit(solution)/shard_map/all_to_all | solution.py:35
  35.7 10.4 %all-to-all-done.1 = bf16[16,64,128]{2,1,0:T(8,128)(2,1)S(1)} async-done(((bf16[16,64,128]{2,1,0:T(8,128)(2,1)}), bf16[16,64,128]{2,1,0:T(8,128)(2,1)S(1)}, u32[]{:S(2)}, u32[]{:S(2)}) %all-to-all-start.1) | async-done | bytes 262176 | tf_op jit(solution)/shard_map/all_to_all | solution.py:35
  46.9 3.4 %all-to-all-start.2 = ((bf16[16,64,128]{2,1,0:T(8,128)(2,1)}), bf16[16,64,128]{2,1,0:T(8,128)(2,1)S(1)}, u32[]{:S(2)}, u32[]{:S(2)}) async-start(bf16[16,64,128]{2,1,0:T(8,128)(2,1)} %broadcast_in_dim.49), calls=%async_computation.2 | async-start | bytes 524288 | tf_op jit(solution)/shard_map/all_to_all | solution.py:21
  50.6 11.4 %all-to-all-done.2 = bf16[16,64,128]{2,1,0:T(8,128)(2,1)S(1)} async-done(((bf16[16,64,128]{2,1,0:T(8,128)(2,1)}), bf16[16,64,128]{2,1,0:T(8,128)(2,1)S(1)}, u32[]{:S(2)}, u32[]{:S(2)}) %all-to-all-start.2) | async-done | bytes 262176 | tf_op jit(solution)/shard_map/all_to_all | solution.py:21
  62.2 1.3 convolution_convert_fusion.1
  63.5 1.3 reshape.211
  64.8 24.5 %all_to_all.30 = bf16[16,1,12,2048]{3,2,1,0:T(8,128)(2,1)S(1)} all-to-all(bf16[16,1,12,2048]{3,2,1,0:T(8,128)(2,1)S(1)} %bitcast.125), channel_id=1, replica_groups=mesh['ep'=16,'tp'=16] {'ep'}, dimensions={0} | all-to-all | bytes 1572864 | tf_op jit(solution)/shard_map/all_to_all | solution.py:120
  89.3 1.0 copy-done.3
  90.3 0.8 fusion.10
  91.1 3.3 %fusion.7 = bf16[1,12,2,16,8,128]{5,4,3,2,1,0:T(8,128)(2,1)S(1)} fusion(bf16[1,448,2048]{2,1,0:T(8,128)(2,1)S(1)} %copy-done, bf16[1,2048,448]{1,2,0:T(8,128)(2,1)} %param.28, bf16[16,1,12,2048]{3,2,1,0:T(8,128)(2,1)} %copy-done.3, f32[16,1,12,448]{3,0,2,1:T(8,128)S(1)} %fusion.10), kind=kOutput, calls=%fused_computation.12 | convolution fusion | flops 705552384 | bytes 5586944 | tf_op jit(solution)/shard_map/secf,efd->secd/dot_general | solution.py:126
  94.4 1.1 copy.73
  95.5 4.0 %all-to-all-start.4 = ((bf16[16,16,1,12,128]{4,1,3,2,0:T(8,128)(2,1)}), bf16[16,16,1,12,128]{4,1,3,2,0:T(8,128)(2,1)S(1)}, u32[]{:S(2)}, u32[]{:S(2)}) async-start(bf16[16,16,1,12,128]{4,1,3,2,0:T(8,128)(2,1)} %bitcast.122), calls=%async_computation.4 | async-start | bytes 1572864 | tf_op jit(solution)/shard_map/all_to_all | solution.py:35
  100.2 22.0 %all-to-all-done.4 = bf16[16,16,1,12,128]{4,1,3,2,0:T(8,128)(2,1)S(1)} async-done(((bf16[16,16,1,12,128]{4,1,3,2,0:T(8,128)(2,1)}), bf16[16,16,1,12,128]{4,1,3,2,0:T(8,128)(2,1)S(1)}, u32[]{:S(2)}, u32[]{:S(2)}) %all-to-all-start.4) | async-done | bytes 786464 | tf_op jit(solution)/shard_map/all_to_all | solution.py:35
  123.1 3.5 %all-to-all-start.5 = ((f32[16,1,12,128]{3,1,2,0:T(1,128)}), f32[16,1,12,128]{3,1,2,0:T(1,128)S(1)}, u32[]{:S(2)}, u32[]{:S(2)}) async-start(f32[16,1,12,128]{3,1,2,0:T(1,128)} %copy.47), calls=%async_computation.5 | async-start | bytes 196608 | tf_op jit(solution)/shard_map/all_to_all | solution.py:128
  126.7 6.6 %all-to-all-done.5 = f32[16,1,12,128]{3,1,2,0:T(1,128)S(1)} async-done(((f32[16,1,12,128]{3,1,2,0:T(1,128)}), f32[16,1,12,128]{3,1,2,0:T(1,128)S(1)}, u32[]{:S(2)}, u32[]{:S(2)}) %all-to-all-start.5) | async-done | bytes 98336 | tf_op jit(solution)/shard_map/all_to_all | solution.py:128
  133.2 1.0 fusion.26
  (53 shorter events, 5.8 us)
Async XLA Ops:
  0.6 90.4 %copy-start = (bf16[1,448,2048]{2,1,0:T(8,128)(2,1)S(1)}, bf16[1,448,2048]{2,1,0:T(8,128)(2,1)}, u32[]{:S(2)}) copy-start(bf16[1,448,2048]{2,1,0:T(8,128)(2,1)} %param.29) | copy-start | bytes 5505028
  0.6 25.6 %copy-start.6 = (bf16[2048,64]{0,1:T(8,128)(2,1)S(1)}, bf16[2048,64]{0,1:T(8,128)(2,1)}, u32[]{:S(2)}) copy-start(bf16[2048,64]{0,1:T(8,128)(2,1)} %param.20) | copy-start | bytes 786436
  0.7 25.8 %copy-start.7 = (bf16[2048,64]{0,1:T(8,128)(2,1)S(1)}, bf16[2048,64]{0,1:T(8,128)(2,1)}, u32[]{:S(2)}) copy-start(bf16[2048,64]{0,1:T(8,128)(2,1)} %param.19) | copy-start | bytes 786436
  2.3 21.6 %all-to-all-start = ((bf16[16,64,128]{2,1,0:T(8,128)(2,1)}), bf16[16,64,128]{2,1,0:T(8,128)(2,1)S(1)}, u32[]{:S(2)}, u32[]{:S(2)}) async-start(bf16[16,64,128]{2,1,0:T(8,128)(2,1)} %broadcast_in_dim.24), calls=%async_computation | async-start | bytes 524288 | tf_op jit(solution)/shard_map/all_to_all | solution.py:21
  23.8 2.9 %copy-start.2 = (f32[64,1,64,128]{3,2,1,0:T(8,128)S(1)}, f32[64,1,64,128]{3,2,1,0:T(8,128)}, u32[]{:S(2)}) copy-start(f32[64,1,64,128]{3,2,1,0:T(8,128)} %param.16) | copy-start | bytes 6291460
  27.5 1.3 copy-start.1
  27.5 2.7 %copy-start.5 = (bf16[2048,128]{1,0:T(8,128)(2,1)S(1)}, bf16[2048,128]{1,0:T(8,128)(2,1)}, u32[]{:S(2)}) copy-start(bf16[2048,128]{1,0:T(8,128)(2,1)} %param.22) | copy-start | bytes 1572868
  27.5 2.9 %copy-start.4 = (bf16[128,2048]{1,0:T(8,128)(2,1)S(1)}, bf16[128,2048]{1,0:T(8,128)(2,1)}, u32[]{:S(2)}) copy-start(bf16[128,2048]{1,0:T(8,128)(2,1)} %param.23) | copy-start | bytes 1572868
  29.8 16.2 %copy-start.8 = (bf16[64,128]{1,0:T(8,128)(2,1)S(1)}, bf16[64,128]{1,0:T(8,128)(2,1)}, u32[]{:S(2)}) copy-start(bf16[64,128]{1,0:T(8,128)(2,1)} %param.15) | copy-start | bytes 49156
  30.4 31.8 %copy-start.9 = (f32[2048]{0:T(1024)S(1)}, f32[2048]{0:T(1024)}, u32[]{:S(2)}) copy-start(f32[2048]{0:T(1024)} %param.24) | copy-start | bytes 24580
  31.5 14.6 %all-to-all-start.1 = ((bf16[16,64,128]{2,1,0:T(8,128)(2,1)}), bf16[16,64,128]{2,1,0:T(8,128)(2,1)S(1)}, u32[]{:S(2)}, u32[]{:S(2)}) async-start(bf16[16,64,128]{2,1,0:T(8,128)(2,1)} %bitcast.124), calls=%async_computation.1 | async-start | bytes 524288 | tf_op jit(solution)/shard_map/all_to_all | solution.py:35
  46.9 15.2 %all-to-all-start.2 = ((bf16[16,64,128]{2,1,0:T(8,128)(2,1)}), bf16[16,64,128]{2,1,0:T(8,128)(2,1)S(1)}, u32[]{:S(2)}, u32[]{:S(2)}) async-start(bf16[16,64,128]{2,1,0:T(8,128)(2,1)} %broadcast_in_dim.49), calls=%async_computation.2 | async-start | bytes 524288 | tf_op jit(solution)/shard_map/all_to_all | solution.py:21
  64.8 25.5 %copy-start.10 = (bf16[1,2048,448]{1,2,0:T(8,128)(2,1)S(1)}, bf16[1,2048,448]{1,2,0:T(8,128)(2,1)}, u32[]{:S(2)}) copy-start(bf16[1,2048,448]{1,2,0:T(8,128)(2,1)} %param.27) | copy-start | bytes 5505028
  89.3 1.0 copy-start.3
  95.5 26.8 %all-to-all-start.4 = ((bf16[16,16,1,12,128]{4,1,3,2,0:T(8,128)(2,1)}), bf16[16,16,1,12,128]{4,1,3,2,0:T(8,128)(2,1)S(1)}, u32[]{:S(2)}, u32[]{:S(2)}) async-start(bf16[16,16,1,12,128]{4,1,3,2,0:T(8,128)(2,1)} %bitcast.122), calls=%async_computation.4 | async-start | bytes 1572864 | tf_op jit(solution)/shard_map/all_to_all | solution.py:35
  123.1 10.1 %all-to-all-start.5 = ((f32[16,1,12,128]{3,1,2,0:T(1,128)}), f32[16,1,12,128]{3,1,2,0:T(1,128)S(1)}, u32[]{:S(2)}, u32[]{:S(2)}) async-start(f32[16,1,12,128]{3,1,2,0:T(1,128)} %copy.47), calls=%async_computation.5 | async-start | bytes 196608 | tf_op jit(solution)/shard_map/all_to_all | solution.py:128
where the time goes:
time: 135 us; the launch traced here: 134 us
  waiting for transfers between devices  61.3 us (45%)
  blocking collectives  24.5 us (18%)
  starting transfers between devices  24.4 us (18%)
  local copies, waits for them, and re-layouts  10.2 us (8%)
  matrix products  9.6 us (7%)
  other arithmetic  2.65 us (2%)
  between operations  1.6 us (1%)
    all_to_all x2, waiting for transfers between devices, sum_at_owner(): lax.all_to_all(blocks, axis, split_axis=0, concat_axis=0, tiled=True)  32.4 us
    all_to_all x1, blocking collectives, on_device(): lax.all_to_all(sent, 'ep', split_axis=0, concat_axis=0, tiled=True)  24.5 us
    all_to_all x2, waiting for transfers between devices, sent_to_all(): return lax.all_to_all(copies, axis, split_axis=0, concat_axis=0, tiled=True)  22.3 us
    all_to_all x2, starting transfers between devices, sent_to_all(): return lax.all_to_all(copies, axis, split_axis=0, concat_axis=0, tiled=True)  13.4 us
    all_to_all x2, starting transfers between devices, sum_at_owner(): lax.all_to_all(blocks, axis, split_axis=0, concat_axis=0, tiled=True)  7.45 us
    all_to_all x1, waiting for transfers between devices, on_device(): lax.all_to_all(reduced, 'ep', split_axis=0, concat_axis=0, tiled=True)  6.57 us
    all_to_all x1, starting transfers between devices, on_device(): lax.all_to_all(reduced, 'ep', split_axis=0, concat_axis=0, tiled=True)  3.51 us
    dot_general x1, matrix products, on_device(): jnp.einsum('secf,efd->secd', hidden, expert_down, preferred_element_type=...  3.29 us
  transfers between devices with their start and end apart: 5, of which 5 were waited for; matrix products, arithmetic and copies ran while one was open for 1% of the time, Pallas kernels for 0%

commit v1 on v0

v1 whole, which is shorter than its diff:
```python
import functools
import jax
import jax.numpy as jnp
from jax import lax
from jax.experimental import pallas as pl
from jax.experimental.pallas import tpu as pltpu
from jax.sharding import PartitionSpec as P

DK = 64
DV = 128
SLOT = 16
EPSILON = 1e-06
F32 = jnp.float32
BF16 = jnp.bfloat16


def near_first(n):
    return sorted(range(1, n), key=lambda d: (min(d, n - d), d))


def layer_kernel(
    nx, ny, nz, cap,
    tokens, prior, decay_in, norm_in, wq, wk, wv, wg, wo, norm_moe,
    routes, route_w, egate, eup, edown,
    out, k_out, v_out,
    decay, tok, wqk_v, wv_v, wg_v, prior_v, nin_v, nmoe_v, rt_v, rw_v,
    q_s, read_s, mix2, wo2, ps, pf, pr, resz, sel, x2, xn, wga, wup, h2, wd2,
    ds, ret, flat, qs, qf, qr,
    ld, ld2,
    p1s, p1r, rls, rlr, wos, wor, wds, wdr, mxs, mxr, p3s, p3r, p4s, p4r,
    p5s, p5r, xls, xlr, hs, hr, p6s, p6r, p7s, p7r,
):
    n_ep = nx * ny
    rows = tokens.shape[0]
    ep = lax.axis_index("ep")
    tp = lax.axis_index("tp")
    z = lax.div(tp, 2)
    c = lax.rem(tp, 2)
    o = 1 - c
    partner = 2 * z + o
    ye = lax.div(ep, nx)
    xe = lax.rem(ep, nx)
    half = nz * 128

    def up_z(d):
        return lax.rem(z + d, nz)

    def down_z(d):
        return lax.rem(z + nz - d, nz)

    def up_ep(d):
        dy, dx = divmod(d, nx)
        return lax.rem(ye + dy, ny) * nx + lax.rem(xe + dx, nx)

    def down_ep(d):
        dy, dx = divmod(d, nx)
        return lax.rem(ye + ny - dy, ny) * nx + lax.rem(xe + nx - dx, nx)

    def hops(d):
        dy, dx = divmod(d, nx)
        return min(dx, nx - dx) + min(dy, ny - dy)

    z_order = near_first(nz)
    ep_order = sorted(range(1, n_ep), key=lambda d: (hops(d), d))

    def remote(src, dst, ss, rs, e, t):
        return pltpu.make_async_remote_copy(
            src_ref=src, dst_ref=dst, send_sem=ss, recv_sem=rs,
            device_id=(e, t), device_id_type=pl.DeviceIdType.MESH,
        )

    sent = []

    def go(copy):
        copy.start()
        sent.append(copy)
        return copy

    def lanes(i):
        return pl.ds(pl.multiple_of(i * 128, 128), 128)

    tok_ld = pltpu.make_async_copy(tokens, tok.at[tp], ld.at[0])
    tok_ld.start()
    barrier = pltpu.get_barrier_semaphore()
    peers = [(ep, partner)] + [(ep, 2 * up_z(d) + c) for d in z_order]
    peers += [(up_ep(d), tp) for d in ep_order]
    flat[...] = jnp.zeros_like(flat)
    xn[...] = jnp.zeros_like(xn)
    for who in peers:
        pl.semaphore_signal(barrier, inc=1, device_id=who, device_id_type=pl.DeviceIdType.MESH)
    rt_block = lanes(lax.div(ep * rows, 128))
    first = [
        (wq, wqk_v.at[0:DK, :]), (wk, wqk_v.at[DK : 2 * DK, :]), (wv, wv_v), (wg, wg_v), (prior, prior_v),
        (decay_in, decay), (norm_in, nin_v), (norm_moe, nmoe_v),
        (routes.at[:, rt_block], rt_v), (route_w.at[:, rt_block], rw_v),
    ]
    first = [pltpu.make_async_copy(a, b, ld.at[i + 1]) for i, (a, b) in enumerate(first)]
    for copy in first:
        copy.start()
    pl.semaphore_wait(barrier, len(peers))
    tok_ld.wait()

    p1 = {}
    for d in z_order:
        p1[d] = go(remote(tok.at[tp], tok.at[tp], p1s.at[d], p1r.at[d], ep, 2 * up_z(d) + c))
    relay = {0: go(remote(tok.at[tp], tok.at[tp], rls.at[0], rlr.at[0], ep, partner))}

    wo_swap = []
    wd_swap = []
    rows_d = edown.shape[0]
    my_wo = pl.ds(pl.multiple_of(c * 128, 128), 128)
    loads = []

    def load(a, b):
        copy = pltpu.make_async_copy(a, b, ld2.at[len(loads)])
        copy.start()
        loads.append(copy)
        return copy

    wo_load = []
    for i in range(nz):
        dst = wo2.at[my_wo, pl.ds(i * 128, 128)]
        wo_load.append(load(wo.at[:, lanes(2 * i + c)], dst))
        wo_swap.append(
            go(remote(wo.at[:, lanes(2 * i + o)], dst, wos.at[i], wor.at[i], ep, partner))
        )
    e_load = []
    for j in range(2 * nz):
        k = (j % 2) * nz + j // 2
        src, dst = pl.ds(j * 128, 128), pl.ds(k * 128, 128)
        e_load.append(load(egate.at[:, src], wga.at[:, dst]))
        e_load.append(load(eup.at[:, src], wup.at[:, dst]))
    d_load = []
    for i in range(nz):
        dst = wd2.at[c, :, pl.ds(i * 128, 128)]
        d_load.append(load(edown.at[:, lanes(2 * i + c)], dst))
        wd_swap.append(
            go(remote(edown.at[:, lanes(2 * i + o)], dst, wds.at[i], wdr.at[i], ep, partner))
        )

    for copy in first:
        copy.wait()

    width = SLOT * n_ep
    side = lax.rem(ep * rows, 128)
    r01 = rt_v[...]
    w01 = rw_v[...]
    r_all, w_all = r01, w01
    for at in range(rows, 128, rows):
        shifted = side == at
        r01 = jnp.where(shifted, jnp.concatenate([r_all[:, at:], r_all[:, :at]], 1), r01)
        w01 = jnp.where(shifted, jnp.concatenate([w_all[:, at:], w_all[:, :at]], 1), w01)
    at = lax.broadcasted_iota(jnp.int32, (width, 128), 0)
    label = at >> 4
    place = (at & (SLOT - 1)).astype(F32)
    m0 = r01[0:1, :] == label
    m1 = r01[1:2, :] == label
    chosen = jnp.where(m0 | m1, 1.0, 0.0)
    before = lax.broadcasted_iota(jnp.int32, (128, 128), 0) < lax.broadcasted_iota(
        jnp.int32, (128, 128), 1
    )
    rank = jnp.dot(
        chosen.astype(BF16), jnp.where(before, 1.0, 0.0).astype(BF16), preferred_element_type=F32
    )
    hit = jnp.where(rank == place, chosen, 0.0)
    picked = hit[:, :rows].astype(BF16)
    weight_t = hit * jnp.where(m0, w01[0:1, :], w01[1:2, :])
    spread = weight_t.T[:rows, :]
    spread_hi = spread.astype(BF16)
    spread_lo = (spread - spread_hi.astype(F32)).astype(BF16)
    spread2 = jnp.concatenate([spread_hi, spread_lo], 0)

    for d in z_order:
        p1[d].wait_recv()
        j = 2 * down_z(d) + c
        relay[d] = go(remote(tok.at[j], tok.at[j], rls.at[d], rlr.at[d], ep, partner))
    for d in [0] + z_order:
        relay[d].wait_recv()

    square = jnp.zeros((rows, 128), F32)
    blocks = [tok[j].astype(F32) for j in range(2 * nz)]
    for block in blocks:
        square += block * block
    factor = lax.rsqrt(jnp.sum(square, -1, keepdims=True) / (2 * half) + EPSILON)
    normed_in = jnp.concatenate(
        [(b * factor * nin_v[j : j + 1, :]).astype(BF16) for j, b in enumerate(blocks)], 1
    )

    def project(weight, across):
        dims = (((1,), (across,)), ((), ()))
        made = lax.dot_general(normed_in, weight[...], dims, preferred_element_type=F32)
        return made.astype(BF16).astype(F32)

    query_key = project(wqk_v, 1)
    query = query_key[:, :DK]
    q_s[...] = query
    keyed = query_key[:, DK:] * DK ** (-0.5)
    valued = project(wv_v, 0)
    gate_pre = project(wg_v, 0)
    k_out[...] = keyed
    v_out[...] = valued

    def group(i, _):
        at8 = pl.ds(pl.multiple_of(i * 8, 8), 8)
        read_s[at8, :] = jnp.sum(prior_v[at8] * q_s[at8, :][:, :, None], 1)
        return 0

    lax.fori_loop(0, rows // 8, group, 0)
    keep = 1.0 - decay[0]
    read = keep * read_s[...] + jnp.sum(query * keyed, -1, keepdims=True) * valued
    centred = read - jnp.mean(read, -1, keepdims=True)
    normed = centred * lax.rsqrt(jnp.mean(centred * centred, -1, keepdims=True) + EPSILON)
    mix2[c] = (gate_pre * jax.nn.sigmoid(gate_pre) * normed).astype(BF16)
    mix = go(remote(mix2.at[c], mix2.at[c], mxs.at[0], mxr.at[0], ep, partner))
    for copy in wo_load:
        copy.wait()
    for copy in wo_swap:
        copy.wait_recv()
    mix.wait_recv()
    mixed = jnp.concatenate([mix2[0], mix2[1]], 1)
    part = jnp.dot(mixed, wo2[...], preferred_element_type=F32)
    for i in range(nz):
        piece = part[:, i * 128 : (i + 1) * 128]
        pf[i] = piece
        ps[i] = piece.astype(BF16)

    p3 = [go(remote(ps.at[up_z(d)], pr.at[d], p3s.at[d], p3r.at[d], ep, 2 * up_z(d) + c)) for d in z_order]
    total = tok[tp].astype(F32) + pf[z]
    for d, copy in zip(z_order, p3):
        copy.wait_recv()
    for d in z_order:
        total += pr[d].astype(F32)
    resid = total.astype(BF16)
    resz[z] = resid
    p4 = [go(remote(resz.at[z], resz.at[z], p4s.at[d], p4r.at[d], ep, 2 * up_z(d) + c)) for d in z_order]
    for copy in p4:
        copy.wait_recv()
    whole = jnp.concatenate([resz[i] for i in range(nz)], 1)
    rows_out = jnp.dot(picked, whole, preferred_element_type=F32).astype(BF16)
    for e in range(n_ep):
        sel[e] = rows_out[e * SLOT : e * SLOT + cap, :]

    p5 = {}
    for d in ep_order:
        e = up_ep(d)
        p5[d] = go(remote(sel.at[e], x2.at[c, d], p5s.at[d], p5r.at[d], e, tp))
    xrelay = {0: go(remote(sel.at[ep], x2.at[c, 0], xls.at[0], xlr.at[0], ep, partner))}
    x2[c, 0] = sel[ep]
    for d in ep_order:
        p5[d].wait_recv()
        mine = x2.at[c, d]
        xrelay[d] = go(remote(mine, mine, xls.at[d], xlr.at[d], ep, partner))
    gains = [nmoe_v[2 * i + s : 2 * i + s + 1, :] for s in range(2) for i in range(nz)]
    gain = jnp.concatenate(gains, 1)
    for d in [0] + ep_order:
        xrelay[d].wait_recv()
        block = jnp.concatenate([x2[0, d], x2[1, d]], 1).astype(F32)
        mean = jnp.sum(block * block, -1, keepdims=True) / (2 * half)
        xn[d * SLOT : d * SLOT + cap, :] = (block * lax.rsqrt(mean + EPSILON) * gain).astype(BF16)

    for copy in e_load:
        copy.wait()
    dims = (((1,), (1,)), ((), ()))
    gate_part = lax.dot_general(xn[...], wga[...], dims, preferred_element_type=F32)
    up_part = lax.dot_general(xn[...], wup[...], dims, preferred_element_type=F32)
    h2[c] = (gate_part * jax.nn.sigmoid(gate_part) * up_part).astype(BF16)
    hid = go(remote(h2.at[c], h2.at[c], hs.at[0], hr.at[0], ep, partner))
    for copy in d_load:
        copy.wait()
    for copy in wd_swap:
        copy.wait_recv()
    hid.wait_recv()
    down = jnp.dot(h2[0], wd2[0], preferred_element_type=F32)
    down += jnp.dot(h2[1], wd2[1], preferred_element_type=F32)
    down = down.astype(BF16)
    for d in range(n_ep):
        ds[d] = down[d * SLOT : d * SLOT + cap, :]

    p6 = {}
    for d in ep_order:
        p6[d] = go(
            remote(ds.at[d], ret.at[ep], p6s.at[d], p6r.at[d], down_ep(d), tp)
        )
    ret[ep] = ds[0]
    for d in ep_order:
        p6[d].wait_recv()
    for e in range(n_ep):
        flat[e * SLOT : e * SLOT + cap, :] = ret[e]
    both = jnp.dot(spread2, flat[...], preferred_element_type=F32)
    weighed = both[:rows, :] + both[rows:, :]
    for i in range(nz):
        piece = weighed[:, i * 128 : (i + 1) * 128]
        qf[i] = piece
        qs[i] = piece.astype(BF16)
    p7 = [go(remote(qs.at[up_z(d)], qr.at[d], p7s.at[d], p7r.at[d], ep, 2 * up_z(d) + c)) for d in z_order]
    total = resz[z].astype(F32) + qf[z]
    for copy in p7:
        copy.wait_recv()
    for d in z_order:
        total += qr[d].astype(F32)
    out[...] = total.astype(BF16)
    for copy in sent:
        copy.wait_send()


def on_device(
    nx, ny, nz,
    tokens, prior_state, decay_rate, norm_in, query_weight, key_weight, value_weight,
    gate_weight, out_weight, norm_moe, routes, route_weight, expert_gate, expert_up, expert_down,
):
    rows = tokens.shape[0]
    n_ep = nx * ny
    width = SLOT * n_ep
    half = nz * 128
    full = 2 * half
    ffe = expert_gate.shape[2]
    cap = (3 * routes.shape[1] * rows + 2 * n_ep - 1) // (2 * n_ep)
    hbm = pl.BlockSpec(memory_space=pl.ANY)
    vmem = pl.BlockSpec(memory_space=pltpu.VMEM)
    scratch = [
        pltpu.SMEM((1,), F32),
        pltpu.VMEM((2 * nz, rows, 128), BF16),
        pltpu.VMEM((2 * DK, full), BF16),
        pltpu.VMEM((full, DV), BF16),
        pltpu.VMEM((full, DV), BF16),
        pltpu.VMEM((rows, DK, DV), F32),
        pltpu.VMEM((2 * nz, 128), F32),
        pltpu.VMEM((2 * nz, 128), F32),
        pltpu.VMEM((2, 128), jnp.int32),
        pltpu.VMEM((2, 128), F32),
        pltpu.VMEM((rows, DK), F32),
        pltpu.VMEM((rows, DV), F32),
        pltpu.VMEM((2, rows, DV), BF16),
        pltpu.VMEM((2 * DV, half), BF16),
        pltpu.VMEM((nz, rows, 128), BF16),
        pltpu.VMEM((nz, rows, 128), F32),
        pltpu.VMEM((nz, rows, 128), BF16),
        pltpu.VMEM((nz, rows, 128), BF16),
        pltpu.VMEM((n_ep, cap, half), BF16),
        pltpu.VMEM((2, n_ep, cap, half), BF16),
        pltpu.VMEM((width, full), BF16),
        pltpu.VMEM((ffe, full), BF16),
        pltpu.VMEM((ffe, full), BF16),
        pltpu.VMEM((2, width, ffe), BF16),
        pltpu.VMEM((2, ffe, half), BF16),
        pltpu.VMEM((n_ep, cap, half), BF16),
        pltpu.VMEM((n_ep, cap, half), BF16),
        pltpu.VMEM((width, half), BF16),
        pltpu.VMEM((nz, rows, 128), BF16),
        pltpu.VMEM((nz, rows, 128), F32),
        pltpu.VMEM((nz, rows, 128), BF16),
        pltpu.SemaphoreType.DMA((11,)),
        pltpu.SemaphoreType.DMA((6 * nz,)),
    ]
    for n in (nz, nz, nz, nz, nz, nz, nz, nz, 1, 1, nz, nz, nz, nz, n_ep, n_ep, n_ep, n_ep, 1, 1, n_ep, n_ep, nz, nz):
        scratch.append(pltpu.SemaphoreType.DMA((n,)))
    next_hidden, keyed, valued = pl.pallas_call(
        functools.partial(layer_kernel, nx, ny, nz, cap),
        out_shape=(
            jax.ShapeDtypeStruct((rows, 128), BF16),
            jax.ShapeDtypeStruct((rows, DK), F32),
            jax.ShapeDtypeStruct((rows, DV), F32),
        ),
        in_specs=[hbm] * 15,
        out_specs=(vmem, vmem, vmem),
        scratch_shapes=scratch,
        compiler_params=pltpu.CompilerParams(
            collective_id=0, has_side_effects=True, vmem_limit_bytes=67043328
        ),
        name="layer",
    )(
        tokens, prior_state.reshape(rows, DK, DV), decay_rate, norm_in.reshape(2 * nz, 128),
        query_weight.T, key_weight.T, value_weight, gate_weight, out_weight,
        norm_moe.reshape(2 * nz, 128), routes.T, route_weight.T,
        expert_gate.reshape(full, ffe).T, expert_up.reshape(full, ffe).T, expert_down.reshape(ffe, full),
    )
    keep = 1.0 - decay_rate[0]
    new_state = keep * prior_state[:, 0] + keyed[:, :, None] * valued[:, None, :]
    return (next_hidden, new_state[:, None])


def solution(mesh):
    n_ep, n_tp = mesh.shape["ep"], mesh.shape["tp"]
    nx = next(i for i in range(1, n_ep + 1) if i * i >= n_ep)
    placed = (
        P("ep", "tp"),
        P("ep", "tp", None, None),
        P("tp"),
        P(),
        P(None, "tp"),
        P(None, "tp"),
        P(None, "tp"),
        P(None, "tp"),
        P("tp", None),
        P(),
        P(),
        P(),
        P("ep", None, "tp"),
        P("ep", None, "tp"),
        P("ep", "tp", None),
    )
    return jax.shard_map(
        functools.partial(on_device, nx, n_ep // nx, n_tp // 2),
        mesh=mesh,
        in_specs=placed,
        out_specs=(P("ep", "tp"), P("ep", "tp", None, None)),
        check_vma=False,
    )
```

time: 135 us -> 67.8 us (0.50)
  Pallas kernels: 0 us -> 62.9 us
  waiting for transfers between devices: 61.3 us -> 0 us
  blocking collectives: 24.5 us -> 0 us
  starting transfers between devices: 24.4 us -> 0 us
  matrix products: 9.6 us -> 0 us
  local copies, waits for them, and re-layouts: 10.2 us -> 0.61 us
    pallas_call x0 -> x1, Pallas kernels: none -> 62.9 us  [on_device(): pl.pallas_call(functools.partial(layer_kernel, nx, ny, nz, cap), out_shap...]
    all_to_all x5 -> x0, waiting for transfers between devices: 61.3 us -> none  [the longest x2 32.4 us: sum_at_owner(): lax.all_to_all(blocks, axis, split_axis=0, concat_axis=0, tiled=True)]
    all_to_all x1 -> x0, blocking collectives: 24.5 us -> none  [on_device(): lax.all_to_all(sent, 'ep', split_axis=0, concat_axis=0, tiled=True)]
    all_to_all x5 -> x0, starting transfers between devices: 24.4 us -> none  [the longest x2 13.4 us: sent_to_all(): return lax.all_to_all(copies, axis, split_axis=0, concat_axis=0, tiled=True)]
    dot_general x10 -> x0, matrix products: 9.6 us -> none  [the longest x1 3.29 us: on_device(): jnp.einsum('secf,efd->secd', hidden, expert_down, preferred_element_type=...]
    reshape x3 -> x0, local copies, waits for them, and re-layouts: 3.1 us -> none  [the longest x2 1.85 us: split_up(): return jnp.moveaxis(array.reshape(*before, peers, -1, *after), dim, 0)]
    broadcast_in_dim x2 -> x0, local copies, waits for them, and re-layouts: 2.37 us -> none  [sent_to_all(): copies = jnp.broadcast_to(array, (lax.axis_size(axis), *array.shape))]
    add x1, other arithmetic: 0.71 us -> 2.93 us  [on_device(): keep * prior_state[:, 0] + keyed[:, :, None] * valued[:, None, :]]
  transfers between devices with their start and end apart: 5 -> 0, of which waited for: 5 -> 0; matrix products, arithmetic and copies ran while one was open for 1% -> 0% of each run, Pallas kernels for 0% -> 0%
where the time goes in v1:
time: 67.8 us; the launch traced here: 67.7 us
  Pallas kernels  62.9 us (93%)
  other arithmetic  2.93 us (4%)
  between operations  1.3 us (2%)
    pallas_call x1, Pallas kernels, on_device(): pl.pallas_call(functools.partial(layer_kernel, nx, ny, nz, cap), out_shap...  62.9 us
    add x1, other arithmetic, on_device(): keep * prior_state[:, 0] + keyed[:, :, None] * valued[:, None, :]  2.93 us

profile of v1, /device:TPU:1, one launch (start us, length us, event | category | flops | bytes accessed | tf_op | source)
XLA Modules:
  0.0 67.7 jit_solution(13090752261059541674)
XLA Ops:
  1.3 62.9 %layer.1 = (bf16[64,128]{1,0:T(8,128)(2,1)}, f32[64,64]{1,0:T(8,128)}, f32[64,128]{1,0:T(8,128)}) custom-call(bf16[64,128]{1,0:T(8,128)(2,1)} %tokens.1, f32[64,64,128]{2,1,0:T(8,128)} %bitcast.15, f32[1]{0:T(128)S(6)} %copy.18.decay_in, f32[16,128]{1,0:T(8,128)} %bitcast.21, bf16[64,2048]{1,0:T(8,128)(2,1)} %bitcast.19, bf16[64,2048]{1,0:T(8,128)(2,1)} %bitcast.20, ...), custom_call_target="tpu_custom_call" | custom-call | tf_op jit(solution)/shard_map/layer/pallas_call | solution.py:357
  64.1 0.0 copy-start
  64.1 2.9 %multiply_add_fusion = f32[64,1,64,128]{3,2,1,0:T(8,128)} fusion(f32[64,1,64,128]{3,2,1,0:T(8,128)} %param.16, f32[64,128]{1,0:T(8,128)} %get-tuple-element.7, f32[64,64]{1,0:T(8,128)} %get-tuple-element.6, f32[]{:T(128)} %bitcast.12), kind=kLoop, calls=%fused_computation | loop fusion | flops 1572864 | bytes 4243460 | tf_op jit(solution)/shard_map/add | solution.py:378
  67.1 0.0 copy-done
  67.1 0.6 copy.19
Async XLA Ops:
  64.1 2.9 %copy-start = (bf16[64,128]{1,0:T(8,128)(2,1)S(1)}, bf16[64,128]{1,0:T(8,128)(2,1)}, u32[]{:S(2)}) copy-start(bf16[64,128]{1,0:T(8,128)(2,1)} %get-tuple-element.10) | copy-start | bytes 49156

commit v2 on v1

v2 whole, which is shorter than its diff:
```python
import functools
import jax
import jax.numpy as jnp
from jax import lax
from jax.experimental import pallas as pl
from jax.experimental.pallas import tpu as pltpu
from jax.sharding import PartitionSpec as P

DK = 64
DV = 128
SLOT = 16
EPSILON = 1e-06
F32 = jnp.float32
BF16 = jnp.bfloat16


def near_first(n):
    return sorted(range(1, n), key=lambda d: (min(d, n - d), d))


def layer_kernel(
    nx, ny, nz, cap,
    tokens, prior, decay_in, norm_in, wq, wk, wv, wg, wo, norm_moe,
    routes, route_w, egate, eup, edown,
    out, k_out, v_out,
    decay, tok_own, tok, wqk_v, wvg_v, prior_v, nin_v, nmoe_v, rt_v, rw_v, keep2,
    q_s, k_s, v_s, k_in, v_in, read_s, wo2, ps, pr, resz, sel, x2, xn, wga, wup, wd2,
    ds, ret, flat, qs, qr,
    ld, p1s, p1r, wds, wdr, p3s, p3r, p4s, p4r, p5s, p5r, p6s, p6r, p6o, p7s, p7r,
):
    n_ep = nx * ny
    rows = tokens.shape[0]
    ep = lax.axis_index("ep")
    tp = lax.axis_index("tp")
    z = lax.div(tp, 2)
    c = lax.rem(tp, 2)
    o = 1 - c
    partner = 2 * z + o
    ye = lax.div(ep, nx)
    xe = lax.rem(ep, nx)
    half = nz * 128

    def up_z(d):
        return lax.rem(z + d, nz)

    def down_z(d):
        return lax.rem(z + nz - d, nz)

    def up_ep(d):
        dy, dx = divmod(d, nx)
        return lax.rem(ye + dy, ny) * nx + lax.rem(xe + dx, nx)

    def down_ep(d):
        dy, dx = divmod(d, nx)
        return lax.rem(ye + ny - dy, ny) * nx + lax.rem(xe + nx - dx, nx)

    def hops(d):
        dy, dx = divmod(d, nx)
        return min(dx, nx - dx) + min(dy, ny - dy)

    z_order = near_first(nz)
    ep_order = sorted(range(1, n_ep), key=lambda d: (hops(d), d))

    def remote(src, dst, ss, rs, e, t):
        return pltpu.make_async_remote_copy(
            src_ref=src, dst_ref=dst, send_sem=ss, recv_sem=rs,
            device_id=(e, t), device_id_type=pl.DeviceIdType.MESH,
        )

    sent = []

    def go(copy):
        copy.start()
        sent.append(copy)
        return copy

    def lanes(i):
        return pl.ds(pl.multiple_of(i * 128, 128), 128)

    barrier = pltpu.get_barrier_semaphore()
    peers = [(ep, partner)]
    peers += [(ep, 2 * up_z(d) + p) for d in z_order for p in range(2)]
    peers += [(up_ep(d), 2 * z + p) for d in ep_order for p in range(2)]
    for who in peers:
        pl.semaphore_signal(barrier, inc=1, device_id=who, device_id_type=pl.DeviceIdType.MESH)
    loads = []

    def load(a, b):
        copy = pltpu.make_async_copy(a, b, ld.at[len(loads)])
        copy.start()
        loads.append(copy)
        return copy

    swaps = []

    def swap(a, b):
        i = len(swaps)
        swaps.append(go(remote(a, b, wds.at[i], wdr.at[i], ep, partner)))
        return swaps[i]

    def part_of(i, size):
        return pl.ds(pl.multiple_of(i * size, size), size)

    part = rows // 2
    hid_rows = edown.shape[0]
    tok_ld = load(tokens, tok_own)
    rt_block = lanes(lax.div(ep * rows, 128))
    small_ld = [
        load(decay_in, decay), load(norm_in, nin_v), load(norm_moe, nmoe_v),
        load(routes.at[:, rt_block], rt_v), load(route_w.at[:, rt_block], rw_v),
    ]
    mine_ld = [
        load(wq, wqk_v.at[c, 0:DK, :]), load(wk, wqk_v.at[c, DK : 2 * DK, :]),
        load(wv, wvg_v.at[:, lanes(2 * c)]), load(wg, wvg_v.at[:, lanes(2 * c + 1)]),
        load(prior.at[part_of(c, part)], prior_v.at[c]),
    ]
    wo_load = load(wo, wo2.at[part_of(c, 128), :])
    flat[...] = jnp.zeros_like(flat)
    xn[...] = jnp.zeros_like(xn)
    for copy in small_ld:
        copy.wait()
    keep2[c] = jnp.full((8, 128), 1.0 - decay[0], F32)
    pl.semaphore_wait(barrier, len(peers))
    tok_ld.wait()

    tok[tp] = tok_own[part_of(c, part), :]
    p1 = {}
    for d in z_order + [0]:
        for p in range(2):
            src = tok_own.at[p * part : (p + 1) * part, :]
            copy = remote(src, tok.at[tp], p1s.at[d, p], p1r.at[d, c], ep, 2 * up_z(d) + p)
            if d:
                go(copy)
            else:
                pl.when(c != p)(copy.start)
    keep_swap = swap(keep2.at[c], keep2.at[c])
    first_swap = [
        swap(wq, wqk_v.at[c, 0:DK, :]), swap(wk, wqk_v.at[c, DK : 2 * DK, :]),
        swap(wv, wvg_v.at[:, lanes(2 * c)]), swap(wg, wvg_v.at[:, lanes(2 * c + 1)]),
        swap(prior.at[part_of(o, part)], prior_v.at[c]),
    ]
    wo_swap = swap(wo, wo2.at[part_of(c, 128), :])
    mine = part_of(c, hid_rows)
    e_load = [load(a, b.at[mine, :]) for a, b in [(egate, wga), (eup, wup), (edown, wd2)]]
    gate_swap = swap(egate, wga.at[mine, :])
    width = SLOT * n_ep
    side = lax.rem(ep * rows, 128)
    r01 = rt_v[...]
    w01 = rw_v[...]
    r_all, w_all = r01, w01
    for at in range(rows, 128, rows):
        shifted = side == at
        r01 = jnp.where(shifted, jnp.concatenate([r_all[:, at:], r_all[:, :at]], 1), r01)
        w01 = jnp.where(shifted, jnp.concatenate([w_all[:, at:], w_all[:, :at]], 1), w01)
    at = lax.broadcasted_iota(jnp.int32, (width, 128), 0)
    label = at >> 4
    place = (at & (SLOT - 1)).astype(F32)
    m0 = r01[0:1, :] == label
    m1 = r01[1:2, :] == label
    chosen = jnp.where(m0 | m1, 1.0, 0.0)
    before = lax.broadcasted_iota(jnp.int32, (128, 128), 0) < lax.broadcasted_iota(
        jnp.int32, (128, 128), 1
    )
    rank = jnp.dot(
        chosen.astype(BF16), jnp.where(before, 1.0, 0.0).astype(BF16), preferred_element_type=F32
    )
    hit = jnp.where(rank == place, chosen, 0.0)
    picked = hit[:, :rows].astype(BF16)
    weight_t = hit * jnp.where(m0, w01[0:1, :], w01[1:2, :])
    spread = weight_t.T[:rows, :]
    spread_hi = spread.astype(BF16)
    spread_lo = (spread - spread_hi.astype(F32)).astype(BF16)
    spread2 = jnp.concatenate([spread_hi, spread_lo], 0)

    for d in [0] + z_order:
        for p in range(2):
            copy = remote(tok.at[0], tok.at[0], p1s.at[d, p], p1r.at[d, p], ep, partner)
            if d:
                copy.wait_recv()
            else:
                pl.when(c != p)(copy.wait_recv)
    for copy in mine_ld:
        copy.wait()
    keep_swap.wait_recv()
    for copy in first_swap:
        copy.wait_recv()

    square = jnp.zeros((part, 128), F32)
    blocks = [tok[j].astype(F32) for j in range(2 * nz)]
    for block in blocks:
        square += block * block
    factor = lax.rsqrt(jnp.sum(square, -1, keepdims=True) / (2 * half) + EPSILON)
    normed_in = jnp.concatenate(
        [(b * factor * nin_v[j : j + 1, :]).astype(BF16) for j, b in enumerate(blocks)], 1
    )
    dims = (((1,), (1,)), ((), ()))
    qk = lax.dot_general(normed_in, wqk_v[...].reshape(4 * DK, 2 * half), dims, preferred_element_type=F32)
    qk = qk.astype(BF16).astype(F32)
    vg = jnp.dot(normed_in, wvg_v[...], preferred_element_type=F32).astype(BF16).astype(F32)
    for h in range(2):
        q_s[h] = qk[:, 2 * h * DK : (2 * h + 1) * DK]
        k_of = qk[:, (2 * h + 1) * DK : (2 * h + 2) * DK] * DK ** (-0.5)
        v_of = vg[:, 2 * h * DV : (2 * h + 1) * DV]
        k_s[h] = jnp.concatenate([k_of, jnp.zeros_like(k_of)], 1)
        v_s[h] = v_of
    def group(i, _):
        h = lax.div(i, part // 8)
        at8 = pl.ds(pl.multiple_of(lax.rem(i, part // 8) * 8, 8), 8)
        read_s[h, at8, :] = jnp.sum(prior_v[h, at8] * q_s[h, at8, :][:, :, None], 1)
        return 0

    lax.fori_loop(0, 2 * part // 8, group, 0)
    sides = []
    for h in range(2):
        v_of = v_s[h]
        q_k = jnp.sum(q_s[h] * k_s[h][:, :DK], -1, keepdims=True)
        read = keep2[h][0:1, :] * read_s[h] + q_k * v_of
        centred = read - jnp.mean(read, -1, keepdims=True)
        normed = centred * lax.rsqrt(jnp.mean(centred * centred, -1, keepdims=True) + EPSILON)
        gate_pre = vg[:, (2 * h + 1) * DV : (2 * h + 2) * DV]
        sides.append((gate_pre * jax.nn.sigmoid(gate_pre) * normed).astype(BF16))
    mixed = jnp.concatenate(sides, 1)
    wo_load.wait()
    wo_swap.wait_recv()
    made = jnp.dot(mixed, wo2[...], preferred_element_type=F32).astype(BF16)
    for j in range(2 * nz):
        ps[j] = made[:, j * 128 : (j + 1) * 128]

    for d in z_order + [0]:
        for p in range(2):
            at = 2 * up_z(d) + p
            copy = remote(ps.at[at], pr.at[c, d], p3s.at[d, p], p3r.at[d, c], ep, at)
            if d:
                go(copy)
            else:
                pl.when(c != p)(copy.start)
    pr[c, 0] = ps[tp]
    k_swap = swap(k_s.at[o], k_in)
    v_swap = swap(v_s.at[o], v_in)
    up_swap = swap(eup, wup.at[mine, :])
    for d in [0] + z_order:
        for p in range(2):
            copy = remote(pr.at[0, 0], pr.at[0, 0], p3s.at[d, p], p3r.at[d, p], ep, partner)
            if d:
                copy.wait_recv()
            else:
                pl.when(c != p)(copy.wait_recv)
    for p in range(2):
        total = tok_own[p * part : (p + 1) * part, :].astype(F32)
        for d in range(nz):
            total += pr[p, d].astype(F32)
        resz[z, p * part : (p + 1) * part, :] = total.astype(BF16)
    p4 = {}
    for d in z_order:
        p4[d] = go(remote(resz.at[z], resz.at[z], p4s.at[d], p4r.at[d], ep, 2 * up_z(d) + c))
    for t in [0] + z_order:
        if t:
            p4[t].wait_recv()
        at = down_z(t)
        rows_out = jnp.dot(picked, resz[at], preferred_element_type=F32).astype(BF16)
        for e in range(n_ep):
            sel[e, t] = rows_out[e * SLOT : e * SLOT + cap, :]
        for d in ep_order:
            e = up_ep(d)
            remote(
                sel.at[e, t], x2.at[c, d // 2, at], p5s.at[d], p5r.at[c, d // 2], e, 2 * z + d % 2
            ).start()

        @pl.when(c == 1)
        def _():
            remote(sel.at[ep, t], x2.at[1, 0, at], p5s.at[0], p5r.at[1, 0], ep, 2 * z).start()

        @pl.when(c == 0)
        def _():
            x2[0, 0, at] = sel[ep, t]

    down_swap = swap(edown, wd2.at[mine, :])
    k_swap.wait_recv()
    v_swap.wait_recv()
    k_out[part_of(c, part), :] = k_s[c][:, :DK]
    v_out[part_of(c, part), :] = v_s[c]
    k_out[part_of(o, part), :] = k_in[:, :DK]
    v_out[part_of(o, part), :] = v_in[...]
    slots = n_ep // 2

    def slot_copy(cc, s):
        return remote(sel.at[0], x2.at[cc, s], p5s.at[0], p5r.at[cc, s], ep, partner)

    for s in range(slots):

        @pl.when((c == 1) | (s > 0))
        def _():
            slot_copy(0, s).wait_recv()

        slot_copy(1, s).wait_recv()
        pieces = [x2[j % 2, s, j // 2] for j in range(2 * nz)]
        block = jnp.concatenate(pieces, 1).astype(F32)
        mean = jnp.sum(block * block, -1, keepdims=True) / (2 * half)
        gain = jnp.concatenate([nmoe_v[j : j + 1, :] for j in range(2 * nz)], 1)
        xn[s * SLOT : s * SLOT + cap, :] = (block * lax.rsqrt(mean + EPSILON) * gain).astype(BF16)

    for copy in e_load:
        copy.wait()
    for copy in (gate_swap, up_swap, down_swap):
        copy.wait_recv()
    gate_part = lax.dot_general(xn[...], wga[...], dims, preferred_element_type=F32)
    up_part = lax.dot_general(xn[...], wup[...], dims, preferred_element_type=F32)
    hidden = (gate_part * jax.nn.sigmoid(gate_part) * up_part).astype(BF16)
    back_order = z_order[::-1] + [0]
    for t in back_order:
        at = up_z(t)
        cols = pl.ds(pl.multiple_of(at * 256, 256), 256)
        down = jnp.dot(hidden, wd2[:, cols], preferred_element_type=F32).astype(BF16)
        for s in range(slots):
            for p in range(2):
                ds[t, s, p] = down[s * SLOT : s * SLOT + cap, p * 128 : (p + 1) * 128]
        for s in range(slots):
            d = 2 * s + c
            dx, dy = lax.rem(d, nx), lax.div(d, nx)
            src = lax.rem(ye + ny - dy, ny) * nx + lax.rem(xe + nx - dx, nx)
            for p in range(2):
                if s == 0:
                    @pl.when(c == 1)
                    def _():
                        remote(ds.at[t, s, p], ret.at[at, ep], p6s.at[s, p], p6r.at[t], src, 2 * z + p).start()

                    if p == 0:

                        @pl.when(c == 0)
                        def _():
                            ret[at, ep] = ds[t, s, p]

                    else:

                        @pl.when(c == 0)
                        def _():
                            remote(ds.at[t, s, p], ret.at[at, ep], p6s.at[s, p], p6o.at[t], ep, 2 * z + 1).start()

                else:
                    remote(ds.at[t, s, p], ret.at[at, ep], p6s.at[s, p], p6r.at[t], src, 2 * z + p).start()

    p7 = []
    total = resz[z].astype(F32)
    for t in back_order:
        at = up_z(t)
        most = pl.ds(0, n_ep - 1)
        remote(ret.at[at, most], ret.at[at, most], p6s.at[0, 0], p6r.at[t], ep, partner).wait_recv()

        @pl.when(c == 1)
        def _():
            remote(ret.at[at, 0], ret.at[at, 0], p6s.at[0, 0], p6o.at[t], ep, partner).wait_recv()

        for e in range(n_ep):
            flat[e * SLOT : e * SLOT + cap, :] = ret[at, e]
        both = jnp.dot(spread2, flat[...], preferred_element_type=F32)
        weighed = both[:rows, :] + both[rows:, :]
        if t:
            qs[t] = weighed.astype(BF16)
            p7.append(go(remote(qs.at[t], qr.at[t], p7s.at[t], p7r.at[t], ep, 2 * at + c)))
        else:
            total += weighed
    for copy in p7:
        copy.wait_recv()
    for d in z_order:
        total += qr[d].astype(F32)
    out[...] = total.astype(BF16)
    for p in range(2):
        copy = remote(tok.at[0], tok.at[0], p1s.at[0, p], p1r.at[0, p], ep, partner)
        pl.when(c != p)(copy.wait_send)
        copy = remote(pr.at[0, 0], pr.at[0, 0], p3s.at[0, p], p3r.at[0, p], ep, partner)
        pl.when(c != p)(copy.wait_send)
    for d in ep_order:
        remote(sel.at[0], x2.at[0, 0], p5s.at[d], p5r.at[0, 0], ep, partner).wait_send()

    @pl.when(c == 1)
    def _():
        remote(sel.at[0], x2.at[0, 0], p5s.at[0], p5r.at[0, 0], ep, partner).wait_send()

    for s in range(slots):
        for p in range(2):
            done = remote(ds.at[:, s, p], ds.at[:, s, p], p6s.at[s, p], p6r.at[0], ep, partner)
            if s == 0 and p == 0:
                pl.when(c == 1)(done.wait_send)
            else:
                done.wait_send()
    for copy in sent:
        copy.wait_send()


def on_device(
    nx, ny, nz,
    tokens, prior_state, decay_rate, norm_in, query_weight, key_weight, value_weight,
    gate_weight, out_weight, norm_moe, routes, route_weight, expert_gate, expert_up, expert_down,
):
    rows = tokens.shape[0]
    n_ep = nx * ny
    width = SLOT * n_ep
    half = nz * 128
    full = 2 * half
    ffe = expert_gate.shape[2]
    cap = (3 * routes.shape[1] * rows + 2 * n_ep - 1) // (2 * n_ep)
    hbm = pl.BlockSpec(memory_space=pl.ANY)
    vmem = pl.BlockSpec(memory_space=pltpu.VMEM)
    part = rows // 2
    scratch = [
        pltpu.SMEM((1,), F32),
        pltpu.VMEM((rows, 128), BF16),
        pltpu.VMEM((2 * nz, part, 128), BF16),
        pltpu.VMEM((2, 2 * DK, full), BF16),
        pltpu.VMEM((full, 4 * DV), BF16),
        pltpu.VMEM((2, part, DK, DV), F32),
        pltpu.VMEM((2 * nz, 128), F32),
        pltpu.VMEM((2 * nz, 128), F32),
        pltpu.VMEM((2, 128), jnp.int32),
        pltpu.VMEM((2, 128), F32),
        pltpu.VMEM((2, 8, 128), F32),
        pltpu.VMEM((2, part, DK), F32),
        pltpu.VMEM((2, part, 2 * DK), F32),
        pltpu.VMEM((2, part, DV), F32),
        pltpu.VMEM((part, 2 * DK), F32),
        pltpu.VMEM((part, DV), F32),
        pltpu.VMEM((2, part, DV), F32),
        pltpu.VMEM((2 * DV, full), BF16),
        pltpu.VMEM((2 * nz, part, 128), BF16),
        pltpu.VMEM((2, nz, part, 128), BF16),
        pltpu.VMEM((nz, rows, 128), BF16),
        pltpu.VMEM((n_ep, nz, cap, 128), BF16),
        pltpu.VMEM((2, n_ep // 2, nz, cap, 128), BF16),
        pltpu.VMEM((width // 2, full), BF16),
        pltpu.VMEM((2 * ffe, full), BF16),
        pltpu.VMEM((2 * ffe, full), BF16),
        pltpu.VMEM((2 * ffe, full), BF16),
        pltpu.VMEM((nz, n_ep // 2, 2, cap, 128), BF16),
        pltpu.VMEM((nz, n_ep, cap, 128), BF16),
        pltpu.VMEM((width, 128), BF16),
        pltpu.VMEM((nz, rows, 128), BF16),
        pltpu.VMEM((nz, rows, 128), BF16),
    ]
    pairs = (n_ep // 2, 2)
    two = (nz, 2)
    for n in (16, two, two, 16, 16, two, two, nz, nz, n_ep, pairs[::-1], pairs, nz, nz, nz, nz):
        scratch.append(pltpu.SemaphoreType.DMA(n if isinstance(n, tuple) else (n,)))
    next_hidden, keyed, valued = pl.pallas_call(
        functools.partial(layer_kernel, nx, ny, nz, cap),
        out_shape=(
            jax.ShapeDtypeStruct((rows, 128), BF16),
            jax.ShapeDtypeStruct((rows, DK), F32),
            jax.ShapeDtypeStruct((rows, DV), F32),
        ),
        in_specs=[hbm] * 15,
        out_specs=(vmem, vmem, vmem),
        scratch_shapes=scratch,
        compiler_params=pltpu.CompilerParams(
            collective_id=0, has_side_effects=True, vmem_limit_bytes=67043328
        ),
        name="layer",
    )(
        tokens, prior_state.reshape(rows, DK, DV), decay_rate, norm_in.reshape(2 * nz, 128),
        query_weight.T, key_weight.T, value_weight, gate_weight, out_weight,
        norm_moe.reshape(2 * nz, 128), routes.T, route_weight.T,
        expert_gate.reshape(full, ffe).T, expert_up.reshape(full, ffe).T, expert_down.reshape(ffe, full),
    )
    keep = 1.0 - decay_rate[0]
    new_state = keep * prior_state[:, 0] + keyed[:, :, None] * valued[:, None, :]
    return (next_hidden, new_state[:, None])


def solution(mesh):
    n_ep, n_tp = mesh.shape["ep"], mesh.shape["tp"]
    nx = next(i for i in range(1, n_ep + 1) if i * i >= n_ep)
    placed = (
        P("ep", "tp"),
        P("ep", "tp", None, None),
        P("tp"),
        P(),
        P(None, "tp"),
        P(None, "tp"),
        P(None, "tp"),
        P(None, "tp"),
        P("tp", None),
        P(),
        P(),
        P(),
        P("ep", None, "tp"),
        P("ep", None, "tp"),
        P("ep", "tp", None),
    )
    return jax.shard_map(
        functools.partial(on_device, nx, n_ep // nx, n_tp // 2),
        mesh=mesh,
        in_specs=placed,
        out_specs=(P("ep", "tp"), P("ep", "tp", None, None)),
        check_vma=False,
    )
```

time: 67.8 us -> 60.4 us (0.89)
  Pallas kernels: 62.9 us -> 55.4 us
    pallas_call x1, Pallas kernels: 62.9 us -> 55.4 us  [on_device(): pl.pallas_call(functools.partial(layer_kernel, nx, ny, nz, cap), out_shap...]
where the time goes in v2:
time: 60.4 us; the launch traced here: 60.2 us
  Pallas kernels  55.4 us (92%)
  other arithmetic  2.93 us (5%)
  between operations  1.3 us (2%)
  local copies, waits for them, and re-layouts  0.61 us (1%)
    pallas_call x1, Pallas kernels, on_device(): pl.pallas_call(functools.partial(layer_kernel, nx, ny, nz, cap), out_shap...  55.4 us
    add x1, other arithmetic, on_device(): keep * prior_state[:, 0] + keyed[:, :, None] * valued[:, None, :]  2.93 us

profile of v2, /device:TPU:1, one launch (start us, length us, event | category | flops | bytes accessed | tf_op | source)
XLA Modules:
  0.0 60.2 jit_solution(2194366971349380235)
XLA Ops:
  1.3 55.4 %layer.1 = (bf16[64,128]{1,0:T(8,128)(2,1)}, f32[64,64]{1,0:T(8,128)}, f32[64,128]{1,0:T(8,128)}) custom-call(bf16[64,128]{1,0:T(8,128)(2,1)} %tokens.1, f32[64,64,128]{2,1,0:T(8,128)} %bitcast.15, f32[1]{0:T(128)S(6)} %copy.18.decay_in, f32[16,128]{1,0:T(8,128)} %bitcast.21, bf16[64,2048]{1,0:T(8,128)(2,1)} %bitcast.19, bf16[64,2048]{1,0:T(8,128)(2,1)} %bitcast.20, ...), custom_call_target="tpu_custom_call" | custom-call | tf_op jit(solution)/shard_map/layer/pallas_call | solution.py:443
  56.7 0.0 copy-start
  56.7 2.9 %multiply_add_fusion = f32[64,1,64,128]{3,2,1,0:T(8,128)} fusion(f32[64,1,64,128]{3,2,1,0:T(8,128)} %param.16, f32[64,128]{1,0:T(8,128)} %get-tuple-element.7, f32[64,64]{1,0:T(8,128)} %get-tuple-element.6, f32[]{:T(128)} %bitcast.12), kind=kLoop, calls=%fused_computation | loop fusion | flops 1572864 | bytes 4243460 | tf_op jit(solution)/shard_map/add | solution.py:464
  59.6 0.0 copy-done
  59.6 0.6 %copy.19 = bf16[64,128]{1,0:T(8,128)(2,1)} copy(bf16[64,128]{1,0:T(8,128)(2,1)S(1)} %copy-done) | data formatting | bytes 32768
Async XLA Ops:
  56.7 2.9 %copy-start = (bf16[64,128]{1,0:T(8,128)(2,1)S(1)}, bf16[64,128]{1,0:T(8,128)(2,1)}, u32[]{:S(2)}) copy-start(bf16[64,128]{1,0:T(8,128)(2,1)} %get-tuple-element.10) | copy-start | bytes 49156

commit v3 on v2

v3 whole, which is shorter than its diff:
```python
import functools
import jax
import jax.numpy as jnp
from jax import lax
from jax.experimental import pallas as pl
from jax.experimental.pallas import tpu as pltpu
from jax.sharding import PartitionSpec as P

DK = 64
DV = 128
SLOT = 16
CUTS = tuple(range(9))
BACK_CUTS = tuple(range(9))
EPSILON = 1e-06
F32 = jnp.float32
BF16 = jnp.bfloat16


def near_first(n):
    return sorted(range(1, n), key=lambda d: (min(d, n - d), d))


def layer_kernel(
    nx, ny, nz, cap,
    tokens, prior, decay_in, norm_in, wq, wk, wv, wg, wo, norm_moe,
    routes, route_w, egate, eup, edown,
    out, k_out, v_out,
    decay, tok_own, tok, wqk_v, wvg_v, prior_v, nin_v, nmoe_v, rt_v, rw_v, keep2,
    halves, q_s, k_s, v_s, k_in, v_in, k_all, wo2, ps, pr, resz, sel, x2, xg, sq, acc, wgu, wd2,
    ds, ret, flat, qs, qr,
    ld, p1s, p1r, wds, wdr, p3s, p3r, p4s, p4r, p5s, p5r, p5o, p6s, p6r, p6o, p7s, p7r,
):
    n_ep = nx * ny
    rows = tokens.shape[0]
    ep = lax.axis_index("ep")
    tp = lax.axis_index("tp")
    z = lax.div(tp, 2)
    c = lax.rem(tp, 2)
    o = 1 - c
    partner = 2 * z + o
    ye = lax.div(ep, nx)
    xe = lax.rem(ep, nx)
    half = nz * 128

    def up_z(d):
        return lax.rem(z + d, nz)

    def down_z(d):
        return lax.rem(z + nz - d, nz)

    def up_ep(d):
        dy, dx = divmod(d, nx)
        return lax.rem(ye + dy, ny) * nx + lax.rem(xe + dx, nx)

    def down_ep(d):
        dy, dx = divmod(d, nx)
        return lax.rem(ye + ny - dy, ny) * nx + lax.rem(xe + nx - dx, nx)

    def hops(d):
        dy, dx = divmod(d, nx)
        return min(dx, nx - dx) + min(dy, ny - dy)

    z_order = near_first(nz)
    ep_order = sorted(range(1, n_ep), key=lambda d: (hops(d), d))

    def remote(src, dst, ss, rs, e, t):
        return pltpu.make_async_remote_copy(
            src_ref=src, dst_ref=dst, send_sem=ss, recv_sem=rs,
            device_id=(e, t), device_id_type=pl.DeviceIdType.MESH,
        )

    sent = []

    def go(copy):
        copy.start()
        sent.append(copy)
        return copy

    def lanes(i):
        return pl.ds(pl.multiple_of(i * 128, 128), 128)

    barrier = pltpu.get_barrier_semaphore()
    slots = n_ep // 2

    def served(s):
        d = 2 * s + c
        dx, dy = lax.rem(d, nx), lax.div(d, nx)
        return lax.rem(ye + ny - dy, ny) * nx + lax.rem(xe + nx - dx, nx)

    def hello(e, t):
        pl.semaphore_signal(barrier, inc=1, device_id=(e, t), device_id_type=pl.DeviceIdType.MESH)

    for p in range(2):
        for d in z_order:
            hello(ep, 2 * up_z(d) + p)
        for s in range(1, slots):
            hello(served(s), 2 * z + p)
        pl.when(c == 1)(functools.partial(hello, served(0), 2 * z + p))
    hello(ep, partner)
    loads = []

    def load(a, b):
        copy = pltpu.make_async_copy(a, b, ld.at[len(loads)])
        copy.start()
        loads.append(copy)
        return copy

    swaps = []

    def swap(a, b):
        i = len(swaps)
        swaps.append(go(remote(a, b, wds.at[i], wdr.at[i], ep, partner)))
        return swaps[i]

    def part_of(i, size):
        return pl.ds(pl.multiple_of(i * size, size), size)

    part = rows // 2
    hid_rows = edown.shape[0]
    tok_ld = load(tokens, tok_own)
    rt_block = lanes(lax.div(ep * rows, 128))
    small_ld = [
        load(decay_in, decay), load(norm_in, nin_v), load(norm_moe, nmoe_v),
        load(routes.at[:, rt_block], rt_v), load(route_w.at[:, rt_block], rw_v),
    ]
    prior_ld = load(prior.at[part_of(c, part)], prior_v.at[c])
    mine_ld = [
        load(wq, wqk_v.at[c, 0:DK, :]), load(wk, wqk_v.at[c, DK : 2 * DK, :]),
        load(wv, wvg_v.at[:, lanes(2 * c)]), load(wg, wvg_v.at[:, lanes(2 * c + 1)]),
    ]
    wo_load = load(wo, wo2.at[part_of(c, 128), :])
    flat[...] = jnp.zeros_like(flat)
    xg[...] = jnp.zeros_like(xg)
    sq[...] = jnp.zeros_like(sq)
    for copy in small_ld:
        copy.wait()
    keep2[c] = jnp.full((8, 128), 1.0 - decay[0], F32)
    pl.semaphore_wait(barrier, 2 * (nz - 1) + n_ep)
    tok_ld.wait()

    tok[tp] = tok_own[part_of(c, part), :]
    p1 = {}
    for d in z_order[::-1] + [0]:
        for p in range(2):
            src = tok_own.at[p * part : (p + 1) * part, :]
            copy = remote(src, tok.at[tp], p1s.at[d, p], p1r.at[d, c], ep, 2 * up_z(d) + p)
            if d:
                go(copy)
            else:
                pl.when(c != p)(copy.start)
    keep_swap = swap(keep2.at[c], keep2.at[c])
    first_swap = [
        swap(wq, wqk_v.at[c, 0:DK, :]), swap(wk, wqk_v.at[c, DK : 2 * DK, :]),
        swap(wv, wvg_v.at[:, lanes(2 * c)]), swap(wg, wvg_v.at[:, lanes(2 * c + 1)]),
    ]
    prior_swap = swap(prior.at[part_of(o, part)], prior_v.at[c])
    wo_swap = swap(wo, wo2.at[part_of(c, 128), :])
    mine = part_of(c, hid_rows)
    gate_rows = mine
    up_rows = pl.ds(pl.multiple_of((2 + c) * hid_rows, hid_rows), hid_rows)
    e_load = [load(egate, wgu.at[gate_rows, :]), load(eup, wgu.at[up_rows, :]), load(edown, wd2.at[mine, :])]
    gate_swap = swap(egate, wgu.at[gate_rows, :])
    up_swap = swap(eup, wgu.at[up_rows, :])
    width = SLOT * n_ep
    side = lax.rem(ep * rows, 128)
    r01 = rt_v[...]
    w01 = rw_v[...]
    r_all, w_all = r01, w01
    for at in range(rows, 128, rows):
        shifted = side == at
        r01 = jnp.where(shifted, jnp.concatenate([r_all[:, at:], r_all[:, :at]], 1), r01)
        w01 = jnp.where(shifted, jnp.concatenate([w_all[:, at:], w_all[:, :at]], 1), w01)
    at = lax.broadcasted_iota(jnp.int32, (width, 128), 0)
    label = at >> 4
    place = (at & (SLOT - 1)).astype(F32)
    m0 = r01[0:1, :] == label
    m1 = r01[1:2, :] == label
    chosen = jnp.where(m0 | m1, 1.0, 0.0)
    before = lax.broadcasted_iota(jnp.int32, (128, 128), 0) < lax.broadcasted_iota(
        jnp.int32, (128, 128), 1
    )
    rank = jnp.dot(
        chosen.astype(BF16), jnp.where(before, 1.0, 0.0).astype(BF16), preferred_element_type=F32
    )
    hit = jnp.where(rank == place, chosen, 0.0)
    picked = hit[:, :rows].astype(BF16)
    weight_t = hit * jnp.where(m0, w01[0:1, :], w01[1:2, :])
    spread = weight_t.T[:rows, :]
    spread_hi = spread.astype(BF16)
    spread_lo = (spread - spread_hi.astype(F32)).astype(BF16)
    spread2 = jnp.concatenate([spread_hi, spread_lo], 0)

    def split(h):
        def some(i, _):
            at4 = pl.ds(i * 4, 4)
            at256 = pl.ds(pl.multiple_of(i * 4 * DK, 4 * DK), 4 * DK)
            value = prior_v[h, at4].reshape(4 * DK, DV)
            high = value.astype(BF16)
            halves[h, at256, 0:DV] = high
            halves[h, at256, DV : 2 * DV] = (value - high.astype(F32)).astype(BF16)
            return 0

        lax.fori_loop(0, part // 4, some, 0)

    prior_ld.wait()
    split(c)
    for copy in mine_ld:
        copy.wait()
    keep_swap.wait_recv()
    for copy in first_swap:
        copy.wait_recv()
    dims = (((1,), (1,)), ((), ()))
    square = jnp.zeros((part, 128), F32)
    qk = jnp.zeros((part, 4 * DK), F32)
    vg = jnp.zeros((part, 4 * DV), F32)
    for d in [0] + z_order:
        for p in range(2):
            copy = remote(tok.at[0], tok.at[0], p1s.at[d, p], p1r.at[d, p], ep, partner)
            if d:
                copy.wait_recv()
            else:
                pl.when(c != p)(copy.wait_recv)
        if d == z_order[len(z_order) // 2]:
            prior_swap.wait_recv()
            split(o)
        at = down_z(d)
        pair = pl.ds(pl.multiple_of(at * 256, 256), 256)
        scaled = []
        for p in range(2):
            block = tok[2 * at + p].astype(F32)
            square += block * block
            scaled.append((block * nin_v[pl.ds(2 * at + p, 1), :]).astype(BF16))
        scaled = jnp.concatenate(scaled, 1)
        qk += lax.dot_general(scaled, wqk_v[:, :, pair].reshape(4 * DK, 256), dims, preferred_element_type=F32)
        vg += jnp.dot(scaled, wvg_v[pair, :], preferred_element_type=F32)
    factor = lax.rsqrt(jnp.sum(square, -1, keepdims=True) / (2 * half) + EPSILON)
    qk = (qk * factor).astype(BF16)
    vg = (vg * factor).astype(BF16).astype(F32)
    wide = lax.broadcasted_iota(jnp.int32, (part, part * DK), 1)
    own_row = lax.div(wide, DK) == lax.broadcasted_iota(jnp.int32, (part, part * DK), 0)
    reads = []
    for h in range(2):
        query = qk[:, 2 * h * DK : (2 * h + 1) * DK].astype(F32)
        k_of = qk[:, (2 * h + 1) * DK : (2 * h + 2) * DK].astype(F32) * DK ** (-0.5)
        q_s[h] = query
        k_s[h] = jnp.concatenate([k_of, jnp.zeros_like(k_of)], 1)
        v_s[h] = vg[:, 2 * h * DV : (2 * h + 1) * DV]
        double = jnp.concatenate([query, query], 1)
        spread_q = jnp.where(own_row, jnp.concatenate([double] * (part // 2), 1), 0.0).astype(BF16)
        both = jnp.dot(spread_q, halves[h], preferred_element_type=F32)
        reads.append(both[:, :DV] + both[:, DV:])
    sides = []
    for h in range(2):
        v_of = v_s[h]
        q_k = jnp.sum(q_s[h] * k_s[h][:, :DK], -1, keepdims=True)
        read = keep2[h][0:1, :] * reads[h] + q_k * v_of
        centred = read - jnp.mean(read, -1, keepdims=True)
        normed = centred * lax.rsqrt(jnp.mean(centred * centred, -1, keepdims=True) + EPSILON)
        gate_pre = vg[:, (2 * h + 1) * DV : (2 * h + 2) * DV]
        sides.append((gate_pre * jax.nn.sigmoid(gate_pre) * normed).astype(BF16))
    mixed = jnp.concatenate(sides, 1)
    wo_load.wait()
    wo_swap.wait_recv()
    made = jnp.dot(mixed, wo2[...], preferred_element_type=F32).astype(BF16)
    for j in range(2 * nz):
        ps[j] = made[:, j * 128 : (j + 1) * 128]

    for d in z_order[::-1] + [0]:
        for p in range(2):
            at = 2 * up_z(d) + p
            copy = remote(ps.at[at], pr.at[c, d], p3s.at[d, p], p3r.at[d, c], ep, at)
            if d:
                go(copy)
            else:
                pl.when(c != p)(copy.start)
    pr[c, 0] = ps[tp]
    k_swap = swap(k_s.at[o], k_in)
    v_swap = swap(v_s.at[o], v_in)
    down_swap = swap(edown, wd2.at[mine, :])
    k_swap.wait_recv()
    v_swap.wait_recv()
    k_all[part_of(c, part), :] = k_s[c]
    k_all[part_of(o, part), :] = k_in[...]
    k_out[...] = k_all[...].T[:DK, :]
    v_out[part_of(c, part), :] = v_s[c]
    v_out[part_of(o, part), :] = v_in[...]
    for d in [0] + z_order:
        for p in range(2):
            copy = remote(pr.at[0, 0], pr.at[0, 0], p3s.at[d, p], p3r.at[d, p], ep, partner)
            if d:
                copy.wait_recv()
            else:
                pl.when(c != p)(copy.wait_recv)
    for p in range(2):
        total = tok_own[p * part : (p + 1) * part, :].astype(F32)
        for d in range(nz):
            total += pr[p, d].astype(F32)
        resz[z, p * part : (p + 1) * part, :] = total.astype(BF16)
    p4 = {}
    for d in z_order:
        p4[d] = go(remote(resz.at[z], resz.at[z], p4s.at[d], p4r.at[d], ep, 2 * up_z(d) + c))
    order = [0] + z_order
    cuts = sorted({min(i, nz) for i in CUTS})
    for g in range(len(cuts) - 1):
        for i in range(cuts[g], cuts[g + 1]):
            if i:
                p4[order[i]].wait_recv()
            rows_out = jnp.dot(picked, resz[down_z(order[i])], preferred_element_type=F32).astype(BF16)
            for e in range(n_ep):
                sel[e, i] = rows_out[e * SLOT : e * SLOT + cap, :]
        span = slice(cuts[g], cuts[g + 1])
        for d in ep_order:
            e = up_ep(d)
            came = p5r.at[g] if d > 1 else p5o.at[g, c]
            remote(sel.at[e, span], x2.at[c, d // 2, span], p5s.at[d], came, e, 2 * z + d % 2).start()

        @pl.when(c == 1)
        def _():
            remote(sel.at[ep, span], x2.at[1, 0, span], p5s.at[0], p5o.at[g, 1], ep, 2 * z).start()

        @pl.when(c == 0)
        def _():
            x2[0, 0, span] = sel[ep, span]

    for copy in e_load[:2]:
        copy.wait()
    gate_swap.wait_recv()
    up_swap.wait_recv()
    for i in range(nz):
        if i in cuts:
            g = cuts.index(i)
            span = slice(cuts[g], cuts[g + 1])
            most = x2.at[:, 1:slots, span]
            remote(most, most, p5s.at[0], p5r.at[g], ep, partner).wait_recv()
            first = [
                remote(x2.at[p, 0, span], x2.at[p, 0, span], p5s.at[0], p5o.at[g, p], ep, partner)
                for p in range(2)
            ]
            pl.when(c == 1)(first[0].wait_recv)
            first[1].wait_recv()
        at = down_z(order[i])
        gains = [nmoe_v[pl.ds(2 * at + p, 1), :] for p in range(2)]
        for s in range(slots):
            span = slice(s * SLOT, s * SLOT + cap)
            both = [x2[p, s, i].astype(F32) for p in range(2)]
            sq[span, :] += both[0] * both[0] + both[1] * both[1]
            for p in range(2):
                xg[span, p * 128 : (p + 1) * 128] = (both[p] * gains[p]).astype(BF16)
        pair = pl.ds(pl.multiple_of(at * 256, 256), 256)
        more = lax.dot_general(xg[...], wgu[:, pair], dims, preferred_element_type=F32)
        if i:
            acc[...] += more
        else:
            acc[...] = more
    scale = lax.rsqrt(jnp.sum(sq[...], -1, keepdims=True) / (2 * half) + EPSILON)
    gate_part = acc[:, : 2 * hid_rows] * scale
    up_part = acc[:, 2 * hid_rows :] * scale
    hidden = (gate_part * jax.nn.sigmoid(gate_part) * up_part).astype(BF16)
    e_load[2].wait()
    down_swap.wait_recv()
    back = z_order[::-1] + [0]
    backs = sorted({min(i, nz) for i in BACK_CUTS})
    far_slots = sorted(range(slots), key=lambda s: (-max(hops(2 * s), hops(2 * s + 1)), s))
    for g in range(len(backs) - 1):
        for i in range(backs[g], backs[g + 1]):
            cols = pl.ds(pl.multiple_of(up_z(back[i]) * 256, 256), 256)
            down = jnp.dot(hidden, wd2[:, cols], preferred_element_type=F32).astype(BF16)
            for s in range(slots):
                for p in range(2):
                    ds[s, p, i] = down[s * SLOT : s * SLOT + cap, p * 128 : (p + 1) * 128]
        span = slice(backs[g], backs[g + 1])
        for s in far_slots:
            for p in range(2):
                home = remote(
                    ds.at[s, p, span], ret.at[ep, span], p6s.at[s, p], p6r.at[g], served(s), 2 * z + p
                )
                if s:
                    home.start()
                    continue
                pl.when(c == 1)(home.start)
                if p == 0:

                    @pl.when(c == 0)
                    def _():
                        ret[ep, span] = ds[0, 0, span]

                else:
                    other = remote(
                        ds.at[s, p, span], ret.at[ep, span], p6s.at[s, p], p6o.at[g], ep, 2 * z + 1
                    )
                    pl.when(c == 0)(other.start)

    p7 = []
    total = resz[z].astype(F32)
    for i in range(nz):
        if i in backs:
            g = backs.index(i)
            span = slice(backs[g], backs[g + 1])
            most = ret.at[0 : n_ep - 1, span]
            remote(most, most, p6s.at[0, 0], p6r.at[g], ep, partner).wait_recv()
            last = remote(ret.at[0, span], ret.at[0, span], p6s.at[0, 0], p6o.at[g], ep, partner)
            pl.when(c == 1)(last.wait_recv)
        for e in range(n_ep):
            flat[e * SLOT : e * SLOT + cap, :] = ret[e, i]
        both = jnp.dot(spread2, flat[...], preferred_element_type=F32)
        weighed = both[:rows, :] + both[rows:, :]
        t = back[i]
        if t:
            qs[t] = weighed.astype(BF16)
            p7.append(go(remote(qs.at[t], qr.at[t], p7s.at[t], p7r.at[t], ep, 2 * up_z(t) + c)))
        else:
            total += weighed
    for copy in p7:
        copy.wait_recv()
    for d in z_order:
        total += qr[d].astype(F32)
    out[...] = total.astype(BF16)
    for p in range(2):
        copy = remote(tok.at[0], tok.at[0], p1s.at[0, p], p1r.at[0, p], ep, partner)
        pl.when(c != p)(copy.wait_send)
        copy = remote(pr.at[0, 0], pr.at[0, 0], p3s.at[0, p], p3r.at[0, p], ep, partner)
        pl.when(c != p)(copy.wait_send)
    for d in ep_order:
        remote(sel.at[0], sel.at[0], p5s.at[d], p5r.at[0], ep, partner).wait_send()

    @pl.when(c == 1)
    def _():
        remote(sel.at[0], sel.at[0], p5s.at[0], p5r.at[0], ep, partner).wait_send()

    for s in range(slots):
        for p in range(2):
            done = remote(ds.at[s, p], ds.at[s, p], p6s.at[s, p], p6r.at[0], ep, partner)
            if s == 0 and p == 0:
                pl.when(c == 1)(done.wait_send)
            else:
                done.wait_send()
    for copy in sent:
        copy.wait_send()


def state_kernel(decay_in, hidden_in, keys_in, values_in, prior_in, hidden_out, state_out, decay, hidden, keys, values, state, sems):
    pieces = 8
    size = values.shape[0] // pieces
    spans = [slice(j * size, (j + 1) * size) for j in range(pieces)]
    small = [(decay_in, decay), (keys_in, keys), (values_in, values), (hidden_in, hidden)]
    loads = [pltpu.make_async_copy(a, b, sems.at[i]) for i, (a, b) in enumerate(small)]
    loads += [pltpu.make_async_copy(prior_in.at[p], state.at[p], sems.at[4 + j]) for j, p in enumerate(spans)]
    for copy in loads:
        copy.start()
    for copy in loads[:4]:
        copy.wait()
    stores = [pltpu.make_async_copy(hidden, hidden_out, sems.at[4 + pieces])]
    stores[0].start()
    keep = 1.0 - decay[0]
    for j, p in enumerate(spans):
        loads[4 + j].wait()
        for row in range(p.start, p.stop):
            state[row] = keep * state[row] + keys[:, row : row + 1] * values[row : row + 1, :]
        stores.append(pltpu.make_async_copy(state.at[p], state_out.at[p], sems.at[5 + pieces + j]))
        stores[-1].start()
    for copy in stores:
        copy.wait()


def on_device(
    nx, ny, nz,
    tokens, prior_state, decay_rate, norm_in, query_weight, key_weight, value_weight,
    gate_weight, out_weight, norm_moe, routes, route_weight, expert_gate, expert_up, expert_down,
):
    rows = tokens.shape[0]
    n_ep = nx * ny
    width = SLOT * n_ep
    half = nz * 128
    full = 2 * half
    ffe = expert_gate.shape[2]
    cap = (3 * routes.shape[1] * rows + 2 * n_ep - 1) // (2 * n_ep)
    hbm = pl.BlockSpec(memory_space=pltpu.HBM)
    vmem = pl.BlockSpec(memory_space=pltpu.VMEM)
    part = rows // 2
    scratch = [
        pltpu.SMEM((1,), F32),
        pltpu.VMEM((rows, 128), BF16),
        pltpu.VMEM((2 * nz, part, 128), BF16),
        pltpu.VMEM((2, 2 * DK, full), BF16),
        pltpu.VMEM((full, 4 * DV), BF16),
        pltpu.VMEM((2, part, DK, DV), F32),
        pltpu.VMEM((2 * nz, 128), F32),
        pltpu.VMEM((2 * nz, 128), F32),
        pltpu.VMEM((2, 128), jnp.int32),
        pltpu.VMEM((2, 128), F32),
        pltpu.VMEM((2, 8, 128), F32),
        pltpu.VMEM((2, part * DK, 2 * DV), BF16),
        pltpu.VMEM((2, part, DK), F32),
        pltpu.VMEM((2, part, 2 * DK), F32),
        pltpu.VMEM((2, part, DV), F32),
        pltpu.VMEM((part, 2 * DK), F32),
        pltpu.VMEM((part, DV), F32),
        pltpu.VMEM((rows, 2 * DK), F32),
        pltpu.VMEM((2 * DV, full), BF16),
        pltpu.VMEM((2 * nz, part, 128), BF16),
        pltpu.VMEM((2, nz, part, 128), BF16),
        pltpu.VMEM((nz, rows, 128), BF16),
        pltpu.VMEM((n_ep, nz, cap, 128), BF16),
        pltpu.VMEM((2, n_ep // 2, nz, cap, 128), BF16),
        pltpu.VMEM((width // 2, 256), BF16),
        pltpu.VMEM((width // 2, 128), F32),
        pltpu.VMEM((width // 2, 4 * ffe), F32),
        pltpu.VMEM((4 * ffe, full), BF16),
        pltpu.VMEM((2 * ffe, full), BF16),
        pltpu.VMEM((n_ep // 2, 2, nz, cap, 128), BF16),
        pltpu.VMEM((n_ep, nz, cap, 128), BF16),
        pltpu.VMEM((width, 128), BF16),
        pltpu.VMEM((nz, rows, 128), BF16),
        pltpu.VMEM((nz, rows, 128), BF16),
    ]
    pairs = (n_ep // 2, 2)
    two = (nz, 2)
    for n in (16, two, two, 16, 16, two, two, nz, nz, n_ep, nz, two, pairs, nz, nz, nz, nz):
        scratch.append(pltpu.SemaphoreType.DMA(n if isinstance(n, tuple) else (n,)))
    next_hidden, keyed, valued = pl.pallas_call(
        functools.partial(layer_kernel, nx, ny, nz, cap),
        out_shape=(
            jax.ShapeDtypeStruct((rows, 128), BF16),
            jax.ShapeDtypeStruct((DK, rows), F32),
            jax.ShapeDtypeStruct((rows, DV), F32),
        ),
        in_specs=[hbm] * 15,
        out_specs=(vmem, vmem, vmem),
        scratch_shapes=scratch,
        compiler_params=pltpu.CompilerParams(
            collective_id=0, has_side_effects=True, vmem_limit_bytes=67043328
        ),
        name="layer",
    )(
        tokens, prior_state.reshape(rows, DK, DV), decay_rate, norm_in.reshape(2 * nz, 128),
        query_weight.T, key_weight.T, value_weight, gate_weight, out_weight,
        norm_moe.reshape(2 * nz, 128), routes.T, route_weight.T,
        expert_gate.reshape(full, ffe).T, expert_up.reshape(full, ffe).T, expert_down.reshape(ffe, full),
    )
    next_hidden, new_state = pl.pallas_call(
        state_kernel,
        out_shape=(jax.ShapeDtypeStruct((rows, 128), BF16), jax.ShapeDtypeStruct((rows, DK, DV), F32)),
        in_specs=[hbm] * 5,
        out_specs=(hbm, hbm),
        scratch_shapes=[
            pltpu.SMEM((1,), F32),
            pltpu.VMEM((rows, 128), BF16),
            pltpu.VMEM((DK, rows), F32),
            pltpu.VMEM((rows, DV), F32),
            pltpu.VMEM((rows, DK, DV), F32),
            pltpu.SemaphoreType.DMA((21,)),
        ],
        compiler_params=pltpu.CompilerParams(vmem_limit_bytes=67043328),
        name="state",
    )(decay_rate, next_hidden, keyed, valued, prior_state.reshape(rows, DK, DV))
    return (next_hidden, new_state[:, None])


def solution(mesh):
    n_ep, n_tp = mesh.shape["ep"], mesh.shape["tp"]
    nx = next(i for i in range(1, n_ep + 1) if i * i >= n_ep)
    placed = (
        P("ep", "tp"),
        P("ep", "tp", None, None),
        P("tp"),
        P(),
        P(None, "tp"),
        P(None, "tp"),
        P(None, "tp"),
        P(None, "tp"),
        P("tp", None),
        P(),
        P(),
        P(),
        P("ep", None, "tp"),
        P("ep", None, "tp"),
        P("ep", "tp", None),
    )
    return jax.shard_map(
        functools.partial(on_device, nx, n_ep // nx, n_tp // 2),
        mesh=mesh,
        in_specs=placed,
        out_specs=(P("ep", "tp"), P("ep", "tp", None, None)),
        check_vma=False,
    )
```

time: 60.4 us -> 55.1 us (0.912)
  other arithmetic: 2.93 us -> 0 us
  Pallas kernels: 55.4 us -> 53.7 us
  local copies, waits for them, and re-layouts: 0.61 us -> 0 us
    pallas_call x1, Pallas kernels: 55.4 us -> 50.6 us  [on_device(): pl.pallas_call(functools.partial(layer_kernel, nx, ny, nz, cap), out_shap...]
    pallas_call x0 -> x1, Pallas kernels: none -> 3.08 us  [on_device(): pl.pallas_call(state_kernel, out_shape=(jax.ShapeDtypeStruct((rows, 128),...]
    add x1 -> x0, other arithmetic: 2.93 us -> none  [on_device(): keep * prior_state[:, 0] + keyed[:, :, None] * valued[:, None, :]]
    unnamed x3 -> x0, local copies, waits for them, and re-layouts: 0.61 us -> none
where the time goes in v3:
time: 55.1 us; the launch traced here: 55 us
  Pallas kernels  53.7 us (97%)
  between operations  1.29 us (2%)
    pallas_call x1, Pallas kernels, on_device(): pl.pallas_call(functools.partial(layer_kernel, nx, ny, nz, cap), out_shap...  50.6 us
    pallas_call x1, Pallas kernels, on_device(): pl.pallas_call(state_kernel, out_shape=(jax.ShapeDtypeStruct((rows, 128),...  3.08 us

profile of v3, /device:TPU:1, one launch (start us, length us, event | category | flops | bytes accessed | tf_op | source)
XLA Modules:
  0.0 55.0 jit_solution(16592757806553318171)
XLA Ops:
  1.3 50.6 %layer.1 = (bf16[64,128]{1,0:T(8,128)(2,1)}, f32[64,64]{1,0:T(8,128)}, f32[64,128]{1,0:T(8,128)}) custom-call(bf16[64,128]{1,0:T(8,128)(2,1)} %tokens.1, f32[64,64,128]{2,1,0:T(8,128)} %bitcast.17, f32[1]{0:T(128)S(6)} %copy.18.decay_in, f32[16,128]{1,0:T(8,128)} %bitcast.24, bf16[64,2048]{1,0:T(8,128)(2,1)} %bitcast.22, bf16[64,2048]{1,0:T(8,128)(2,1)} %bitcast.23, ...), custom_call_target="tpu_custom_call" | custom-call | tf_op jit(solution)/shard_map/layer/pallas_call | solution.py:520
  51.9 3.1 %state.1 = (bf16[64,128]{1,0:T(8,128)(2,1)}, f32[64,64,128]{2,1,0:T(8,128)}) custom-call(f32[1]{0:T(128)S(6)} %copy.18.decay_in, bf16[64,128]{1,0:T(8,128)(2,1)} %get-tuple-element.7.hidden_in, f32[64,64]{1,0:T(8,128)} %get-tuple-element.8.keys_in, f32[64,128]{1,0:T(8,128)} %get-tuple-element.9.values_in, f32[64,64,128]{2,1,0:T(8,128)} %bitcast.18), custom_call_target="tpu_custom_call" | custom-call | tf_op jit(solution)/shard_map/state/pallas_call | solution.py:540

commit v4 on v3

v4 whole, which is shorter than its diff:
```python
import functools
import jax
import jax.numpy as jnp
from jax import lax
from jax.experimental import pallas as pl
from jax.experimental.pallas import tpu as pltpu
from jax.sharding import PartitionSpec as P

DK = 64
DV = 128
SLOT = 16
CUTS = tuple(range(9))
BACK_CUTS = tuple(range(9))
JOINS = tuple(range(1, 9))
EPSILON = 1e-06
F32 = jnp.float32
BF16 = jnp.bfloat16


def near_first(n):
    return sorted(range(1, n), key=lambda d: (min(d, n - d), d))


def layer_kernel(
    nx, ny, nz, cap,
    tokens, prior, decay_in, norm_in, wq, wk, wv, wg, wo, norm_moe,
    routes, route_w, egate, eup, edown,
    out_hbm,
    out,
    decay, tok_own, tok, wqk_v, wvg_v, prior_v, norms, rt_v, rw_v, keep2,
    halves, q_s, k_s, v_s, kv_in, k_all, wo2, ps, pr, resz, sel, x2, xg, sq, acc, wgu, wd2,
    ds, ret, flat, qs, qr,
    ld, p1s, p1r, wds, wdr, p3s, p3r, p4s, p4r, p5s, p5r, p6s, p6r, p7s, p7r,
):
    n_ep = nx * ny
    rows = tokens.shape[0]
    nin_v, nmoe_v = norms.at[0], norms.at[1]
    ep = lax.axis_index("ep")
    tp = lax.axis_index("tp")
    z = lax.div(tp, 2)
    c = lax.rem(tp, 2)
    o = 1 - c
    partner = 2 * z + o
    ye = lax.div(ep, nx)
    xe = lax.rem(ep, nx)
    half = nz * 128

    def up_z(d):
        return lax.rem(z + d, nz)

    def down_z(d):
        return lax.rem(z + nz - d, nz)

    def up_ep(d):
        dy, dx = divmod(d, nx)
        return lax.rem(ye + dy, ny) * nx + lax.rem(xe + dx, nx)

    def down_ep(d):
        dy, dx = divmod(d, nx)
        return lax.rem(ye + ny - dy, ny) * nx + lax.rem(xe + nx - dx, nx)

    def hops(d):
        dy, dx = divmod(d, nx)
        return min(dx, nx - dx) + min(dy, ny - dy)

    z_order = near_first(nz)
    ep_order = sorted(range(1, n_ep), key=lambda d: (hops(d), d))

    def remote(src, dst, ss, rs, e, t):
        return pltpu.make_async_remote_copy(
            src_ref=src, dst_ref=dst, send_sem=ss, recv_sem=rs,
            device_id=(e, t), device_id_type=pl.DeviceIdType.MESH,
        )

    def go(copy):
        copy.start()
        return copy

    def arrived(ref, sem):
        remote(ref, ref, sem, sem, ep, partner).wait_recv()

    def left(ref, sem):
        remote(ref, ref, sem, sem, ep, partner).wait_send()

    def lanes(i):
        return pl.ds(pl.multiple_of(i * 128, 128), 128)

    barrier = pltpu.get_barrier_semaphore()
    slots = n_ep // 2

    def served(s):
        d = 2 * s + c
        dx, dy = lax.rem(d, nx), lax.div(d, nx)
        return lax.rem(ye + ny - dy, ny) * nx + lax.rem(xe + nx - dx, nx)

    def hello(e, t):
        pl.semaphore_signal(barrier, inc=1, device_id=(e, t), device_id_type=pl.DeviceIdType.MESH)

    for p in range(2):
        for d in z_order:
            hello(ep, 2 * up_z(d) + p)
        for s in range(1, slots):
            hello(served(s), 2 * z + p)
        pl.when(c == 1)(functools.partial(hello, served(0), 2 * z + p))
    hello(ep, partner)
    def load(i, a, b):
        return go(pltpu.make_async_copy(a, b, ld.at[i]))

    def loaded(i, ref):
        pltpu.make_async_copy(ref, ref, ld.at[i]).wait()

    def swap(i, j, a, b):
        return go(remote(a, b, wds.at[i], wdr.at[j], ep, partner))

    def part_of(i, size):
        return pl.ds(pl.multiple_of(i * size, size), size)

    part = rows // 2
    hid_rows = edown.shape[0]
    tok_ld = load(0, tokens, tok_own)
    rt_block = lanes(lax.div(ep * rows, 128))
    load(1, decay_in, decay)
    load(2, norm_in, nin_v)
    load(2, norm_moe, nmoe_v)
    load(3, routes.at[:, rt_block], rt_v)
    load(4, route_w.at[:, rt_block], rw_v)
    load(5, prior.at[part_of(c, part)], prior_v.at[c])
    load(6, wq, wqk_v.at[c, 0:DK, :])
    load(6, wk, wqk_v.at[c, DK : 2 * DK, :])
    load(7, wv, wvg_v.at[:, lanes(2 * c)])
    load(7, wg, wvg_v.at[:, lanes(2 * c + 1)])
    load(8, wo, wo2.at[part_of(c, 128), :])
    flat[...] = jnp.zeros_like(flat)
    xg[...] = jnp.zeros_like(xg)
    sq[...] = jnp.zeros_like(sq)
    pl.semaphore_wait(barrier, 2 * (nz - 1) + n_ep)
    tok_ld.wait()

    tok[tp] = tok_own[part_of(c, part), :]
    p1 = {}
    for d in z_order[::-1] + [0]:
        for p in range(2):
            src = tok_own.at[p * part : (p + 1) * part, :]
            copy = remote(src, tok.at[tp], p1s.at[0], p1r.at[d], ep, 2 * up_z(d) + p)
            if d:
                go(copy)
            else:
                pl.when(c != p)(copy.start)
    loaded(1, decay)
    loaded(2, norms)
    loaded(3, rt_v)
    loaded(4, rw_v)
    keep2[c] = jnp.full((8, 128), 1.0 - decay[0], F32)
    swap(0, 0, keep2.at[c], keep2.at[c])
    swap(1, 1, wq, wqk_v.at[c, 0:DK, :])
    swap(1, 1, wk, wqk_v.at[c, DK : 2 * DK, :])
    swap(1, 1, wv, wvg_v.at[:, lanes(2 * c)])
    swap(1, 1, wg, wvg_v.at[:, lanes(2 * c + 1)])
    swap(4, 2, prior.at[part_of(o, part)], prior_v.at[c])
    swap(5, 3, wo, wo2.at[part_of(c, 128), :])
    mine = part_of(c, hid_rows)
    up_rows = part_of(2 + c, hid_rows)
    load(9, egate, wgu.at[mine, :])
    load(9, eup, wgu.at[up_rows, :])
    load(10, edown, wd2.at[mine, :])
    swap(2, 4, egate, wgu.at[mine, :])
    swap(2, 4, eup, wgu.at[up_rows, :])
    width = SLOT * n_ep
    side = lax.rem(ep * rows, 128)
    r01 = rt_v[...]
    w01 = rw_v[...]
    r_all, w_all = r01, w01
    for at in range(rows, 128, rows):
        shifted = side == at
        r01 = jnp.where(shifted, jnp.concatenate([r_all[:, at:], r_all[:, :at]], 1), r01)
        w01 = jnp.where(shifted, jnp.concatenate([w_all[:, at:], w_all[:, :at]], 1), w01)
    at = lax.broadcasted_iota(jnp.int32, (width, 128), 0)
    label = at >> 4
    place = (at & (SLOT - 1)).astype(F32)
    m0 = r01[0:1, :] == label
    m1 = r01[1:2, :] == label
    chosen = jnp.where(m0 | m1, 1.0, 0.0)
    before = lax.broadcasted_iota(jnp.int32, (128, 128), 0) < lax.broadcasted_iota(
        jnp.int32, (128, 128), 1
    )
    rank = jnp.dot(
        chosen.astype(BF16), jnp.where(before, 1.0, 0.0).astype(BF16), preferred_element_type=F32
    )
    hit = jnp.where(rank == place, chosen, 0.0)
    picked = hit[:, :rows].astype(BF16)
    weight_t = hit * jnp.where(m0, w01[0:1, :], w01[1:2, :])
    spread = weight_t.T[:rows, :]
    spread_hi = spread.astype(BF16)
    spread_lo = (spread - spread_hi.astype(F32)).astype(BF16)
    spread2 = jnp.concatenate([spread_hi, spread_lo], 0)

    def split(h):
        def some(i, _):
            at4 = pl.ds(i * 4, 4)
            at256 = pl.ds(pl.multiple_of(i * 4 * DK, 4 * DK), 4 * DK)
            value = prior_v[h, at4].reshape(4 * DK, DV)
            high = value.astype(BF16)
            halves[h, at256, 0:DV] = high
            halves[h, at256, DV : 2 * DV] = (value - high.astype(F32)).astype(BF16)
            return 0

        lax.fori_loop(0, part // 4, some, 0)

    loaded(5, prior_v.at[c])
    split(c)
    loaded(6, wqk_v.at[c])
    loaded(7, wvg_v.at[:, part_of(c, 256)])
    arrived(keep2.at[o], wdr.at[0])
    arrived(wvg_v.at[0 : 3 * half // 2, :], wdr.at[1])
    dims = (((1,), (1,)), ((), ()))
    square = jnp.zeros((part, 128), F32)
    qk = jnp.zeros((part, 4 * DK), F32)
    vg = jnp.zeros((part, 4 * DV), F32)
    order = [0] + z_order
    for first_at in range(0, nz, 2):
        if first_at + 2 >= nz:
            arrived(prior_v.at[o], wdr.at[2])
            split(o)
        scaled, wqk_part, wvg_part = [], [], []
        for d in order[first_at : first_at + 2]:
            arrived(tok.at[0 : 2 if d else 1], p1r.at[d])
            at = down_z(d)
            pair = pl.ds(pl.multiple_of(at * 256, 256), 256)
            for p in range(2):
                block = tok[2 * at + p].astype(F32)
                square += block * block
                scaled.append((block * nin_v[pl.ds(2 * at + p, 1), :]).astype(BF16))
            wqk_part.append(wqk_v[:, :, pair].reshape(4 * DK, 256))
            wvg_part.append(wvg_v[pair, :])
        scaled = jnp.concatenate(scaled, 1)
        qk += lax.dot_general(scaled, jnp.concatenate(wqk_part, 1), dims, preferred_element_type=F32)
        vg += jnp.dot(scaled, jnp.concatenate(wvg_part, 0), preferred_element_type=F32)
    factor = lax.rsqrt(jnp.sum(square, -1, keepdims=True) / (2 * half) + EPSILON)
    qk = (qk * factor).astype(BF16)
    vg = (vg * factor).astype(BF16).astype(F32)
    across = lax.broadcasted_iota(jnp.int32, (part, part * DK), 1)
    own_row = lax.div(across, DK) == lax.broadcasted_iota(jnp.int32, (part, part * DK), 0)
    reads = []
    for h in range(2):
        query = qk[:, 2 * h * DK : (2 * h + 1) * DK].astype(F32)
        k_of = qk[:, (2 * h + 1) * DK : (2 * h + 2) * DK].astype(F32) * DK ** (-0.5)
        q_s[h] = query
        k_s[h] = jnp.concatenate([k_of, jnp.zeros_like(k_of)], 1)
        v_s[h] = vg[:, 2 * h * DV : (2 * h + 1) * DV]
        double = jnp.concatenate([query, query], 1)
        spread_q = jnp.where(own_row, jnp.concatenate([double] * (part // 2), 1), 0.0).astype(BF16)
        both = jnp.dot(spread_q, halves[h], preferred_element_type=F32)
        reads.append(both[:, :DV] + both[:, DV:])
    sides = []
    for h in range(2):
        v_of = v_s[h]
        q_k = jnp.sum(q_s[h] * k_s[h][:, :DK], -1, keepdims=True)
        read = keep2[h][0:1, :] * reads[h] + q_k * v_of
        centred = read - jnp.mean(read, -1, keepdims=True)
        normed = centred * lax.rsqrt(jnp.mean(centred * centred, -1, keepdims=True) + EPSILON)
        gate_pre = vg[:, (2 * h + 1) * DV : (2 * h + 2) * DV]
        sides.append((gate_pre * jax.nn.sigmoid(gate_pre) * normed).astype(BF16))
    mixed = jnp.concatenate(sides, 1)
    loaded(8, wo2.at[part_of(c, 128), :])
    arrived(wo2.at[part_of(o, 128), :], wdr.at[3])
    made = jnp.dot(mixed, wo2[...], preferred_element_type=F32).astype(BF16)
    for j in range(2 * nz):
        ps[j] = made[:, j * 128 : (j + 1) * 128]

    for d in z_order[::-1] + [0]:
        for p in range(2):
            at = 2 * up_z(d) + p
            copy = remote(ps.at[at], pr.at[c, d], p3s.at[0], p3r.at[0], ep, at)
            if d:
                go(copy)
            else:
                pl.when(c != p)(copy.start)
    pr[c, 0] = ps[tp]
    swap(3, 5, k_s.at[o], kv_in.at[0])
    swap(3, 5, v_s.at[o], kv_in.at[1])
    swap(2, 6, edown, wd2.at[mine, :])
    arrived(kv_in, wdr.at[5])
    k_all[part_of(c, part), :] = k_s[c]
    k_all[part_of(o, part), :] = kv_in[0]
    out[:, 256:384] = jnp.concatenate([k_all[...].T[:DK, :], jnp.zeros((DK, 128 - rows), F32)], 1)
    out[part_of(c, part), 128:256] = v_s[c]
    out[part_of(o, part), 128:256] = kv_in[1]
    arrived(ps.at[0 : 2 * nz - 1], p3r.at[0])
    for p in range(2):
        total = tok_own[p * part : (p + 1) * part, :].astype(F32)
        for d in range(nz):
            total += pr[p, d].astype(F32)
        resz[z, p * part : (p + 1) * part, :] = total.astype(BF16)
    p4 = {}
    for d in z_order:
        p4[d] = go(remote(resz.at[z], resz.at[z], p4s.at[0], p4r.at[d], ep, 2 * up_z(d) + c))
    cuts = sorted({min(i, nz) for i in CUTS})
    for g in range(len(cuts) - 1):
        for i in range(cuts[g], cuts[g + 1]):
            if i:
                p4[order[i]].wait_recv()
            rows_out = jnp.dot(picked, resz[down_z(order[i])], preferred_element_type=F32).astype(BF16)
            for e in range(n_ep):
                sel[e, i] = rows_out[e * SLOT : e * SLOT + cap, :]
        span = slice(cuts[g], cuts[g + 1])
        for d in ep_order:
            e = up_ep(d)
            remote(
                sel.at[e, span], x2.at[c, d // 2, span], p5s.at[0], p5r.at[g], e, 2 * z + d % 2
            ).start()

        @pl.when(c == 1)
        def _():
            remote(sel.at[ep, span], x2.at[1, 0, span], p5s.at[0], p5r.at[g], ep, 2 * z).start()

        @pl.when(c == 0)
        def _():
            x2[0, 0, span] = sel[ep, span]

    loaded(9, wgu.at[0 : 2 * hid_rows, :])
    arrived(wgu.at[0 : 2 * hid_rows, :], wdr.at[4])
    joins = {min(i, nz) for i in JOINS}
    first_join, wide = True, []
    for i in range(nz):
        if i in cuts:
            g = cuts.index(i)
            span = slice(cuts[g], cuts[g + 1])
            pl.when(c == 1)(functools.partial(arrived, sel.at[:, span], p5r.at[g]))
            pl.when(c == 0)(functools.partial(arrived, sel.at[0 : n_ep - 1, span], p5r.at[g]))
        at = down_z(order[i])
        gains = [nmoe_v[pl.ds(2 * at + p, 1), :] for p in range(2)]
        for s in range(slots):
            span = slice(s * SLOT, s * SLOT + cap)
            both = [x2[p, s, i].astype(F32) for p in range(2)]
            sq[span, :] += both[0] * both[0] + both[1] * both[1]
            for p in range(2):
                lane = (2 * len(wide) + p) * 128
                xg[span, lane : lane + 128] = (both[p] * gains[p]).astype(BF16)
        wide.append(wgu[:, pl.ds(pl.multiple_of(at * 256, 256), 256)])
        if i + 1 in joins:
            used = len(wide) * 256
            more = lax.dot_general(
                xg[:, :used], jnp.concatenate(wide, 1), dims, preferred_element_type=F32
            )
            if first_join:
                acc[...] = more
            else:
                acc[...] += more
            first_join, wide = False, []
    scale = lax.rsqrt(jnp.sum(sq[...], -1, keepdims=True) / (2 * half) + EPSILON)
    gate_part = acc[:, : 2 * hid_rows] * scale
    up_part = acc[:, 2 * hid_rows :] * scale
    hidden = (gate_part * jax.nn.sigmoid(gate_part) * up_part).astype(BF16)
    loaded(10, wd2.at[mine, :])
    arrived(wd2.at[mine, :], wdr.at[6])
    back = z_order[::-1] + [0]
    backs = sorted({min(i, nz) for i in BACK_CUTS})
    far_slots = sorted(range(slots), key=lambda s: (-max(hops(2 * s), hops(2 * s + 1)), s))
    for g in range(len(backs) - 1):
        for i in range(backs[g], backs[g + 1]):
            cols = pl.ds(pl.multiple_of(up_z(back[i]) * 256, 256), 256)
            down = jnp.dot(hidden, wd2[:, cols], preferred_element_type=F32).astype(BF16)
            for s in range(slots):
                for p in range(2):
                    ds[s, p, i] = down[s * SLOT : s * SLOT + cap, p * 128 : (p + 1) * 128]
        span = slice(backs[g], backs[g + 1])
        for s, p in [(s, (p + g) % 2) for s in far_slots[g:] + far_slots[:g] for p in range(2)]:
            if True:
                home = remote(
                    ds.at[s, p, span], ret.at[ep, span], p6s.at[0], p6r.at[g], served(s), 2 * z + p
                )
                if s:
                    home.start()
                    continue
                pl.when(c == 1)(home.start)
                if p == 0:

                    @pl.when(c == 0)
                    def _():
                        ret[ep, span] = ds[0, 0, span]

                else:
                    other = remote(
                        ds.at[s, p, span], ret.at[ep, span], p6s.at[0], p6r.at[g], ep, 2 * z + 1
                    )
                    pl.when(c == 0)(other.start)

    total = resz[z].astype(F32)
    for i in range(nz):
        if i in backs:
            g = backs.index(i)
            span = slice(backs[g], backs[g + 1])
            pl.when(c == 1)(functools.partial(arrived, ret.at[:, span], p6r.at[g]))
            pl.when(c == 0)(functools.partial(arrived, ret.at[0 : n_ep - 1, span], p6r.at[g]))
        for e in range(n_ep):
            flat[e * SLOT : e * SLOT + cap, :] = ret[e, i]
        both = jnp.dot(spread2, flat[...], preferred_element_type=F32)
        weighed = both[:rows, :] + both[rows:, :]
        t = back[i]
        if t:
            qs[t] = weighed.astype(BF16)
            go(remote(qs.at[t], qr.at[t], p7s.at[0], p7r.at[0], ep, 2 * up_z(t) + c))
        else:
            total += weighed
    arrived(qr.at[1:nz], p7r.at[0])
    for d in z_order:
        total += qr[d].astype(F32)
    out[:, :128] = total.astype(BF16).astype(F32)
    load(11, out.at[:, 0:128], out_hbm.at[:, 0:128])
    load(11, out.at[:, 128:384], out_hbm.at[:, 128:384])
    left(ps.at[0 : 2 * nz - 1], p1s.at[0])
    left(ps.at[0 : 2 * nz - 1], p3s.at[0])
    left(resz.at[1:nz], p4s.at[0])
    left(qs.at[1:nz], p7s.at[0])
    left(keep2.at[0], wds.at[0])
    left(wvg_v.at[0 : 3 * half // 2, :], wds.at[1])
    left(prior_v.at[0], wds.at[4])
    left(wo2.at[part_of(c, 128), :], wds.at[5])
    left(wgu.at[0 : 3 * hid_rows, :], wds.at[2])
    left(kv_in, wds.at[3])
    for ref, sem in ((sel, p5s), (ds, p6s)):
        pl.when(c == 1)(functools.partial(left, ref, sem.at[0]))
        pl.when(c == 0)(functools.partial(left, sel.at[0 : n_ep - 1], sem.at[0]))
    loaded(11, out)


def state_kernel(decay, made, prior, hidden_out, state_out, hidden, state, sems):
    pieces = 8
    size = state.shape[0] // pieces
    hidden[...] = made[:, :128].astype(BF16)
    stores = [pltpu.make_async_copy(hidden, hidden_out, sems.at[pieces])]
    stores[0].start()
    keep = 1.0 - decay[0]
    for j in range(pieces):
        for row in range(j * size, (j + 1) * size):
            key, value = made[:, 256 + row : 257 + row], made[row : row + 1, 128:256]
            state[row] = keep * prior[row] + key * value
        span = slice(j * size, (j + 1) * size)
        stores.append(pltpu.make_async_copy(state.at[span], state_out.at[span], sems.at[j]))
        stores[-1].start()
    for copy in stores:
        copy.wait()


def on_device(
    nx, ny, nz,
    tokens, prior_state, decay_rate, norm_in, query_weight, key_weight, value_weight,
    gate_weight, out_weight, norm_moe, routes, route_weight, expert_gate, expert_up, expert_down,
):
    rows = tokens.shape[0]
    n_ep = nx * ny
    width = SLOT * n_ep
    half = nz * 128
    full = 2 * half
    ffe = expert_gate.shape[2]
    cap = (3 * routes.shape[1] * rows + 2 * n_ep - 1) // (2 * n_ep)
    hbm = pl.BlockSpec(memory_space=pltpu.HBM)
    vmem = pl.BlockSpec(memory_space=pltpu.VMEM)
    part = rows // 2
    scratch = [
        pltpu.VMEM((rows, 384), F32),
        pltpu.SMEM((1,), F32),
        pltpu.VMEM((rows, 128), BF16),
        pltpu.VMEM((2 * nz, part, 128), BF16),
        pltpu.VMEM((2, 2 * DK, full), BF16),
        pltpu.VMEM((full, 4 * DV), BF16),
        pltpu.VMEM((2, part, DK, DV), F32),
        pltpu.VMEM((2, 2 * nz, 128), F32),
        pltpu.VMEM((2, 128), jnp.int32),
        pltpu.VMEM((2, 128), F32),
        pltpu.VMEM((2, 8, 128), F32),
        pltpu.VMEM((2, part * DK, 2 * DV), BF16),
        pltpu.VMEM((2, part, DK), F32),
        pltpu.VMEM((2, part, 2 * DK), F32),
        pltpu.VMEM((2, part, DV), F32),
        pltpu.VMEM((2, part, DV), F32),
        pltpu.VMEM((rows, 2 * DK), F32),
        pltpu.VMEM((2 * DV, full), BF16),
        pltpu.VMEM((2 * nz, part, 128), BF16),
        pltpu.VMEM((2, nz, part, 128), BF16),
        pltpu.VMEM((nz, rows, 128), BF16),
        pltpu.VMEM((n_ep, nz, cap, 128), BF16),
        pltpu.VMEM((2, n_ep // 2, nz, cap, 128), BF16),
        pltpu.VMEM((width // 2, 1024), BF16),
        pltpu.VMEM((width // 2, 128), F32),
        pltpu.VMEM((width // 2, 4 * ffe), F32),
        pltpu.VMEM((4 * ffe, full), BF16),
        pltpu.VMEM((2 * ffe, full), BF16),
        pltpu.VMEM((n_ep // 2, 2, nz, cap, 128), BF16),
        pltpu.VMEM((n_ep, nz, cap, 128), BF16),
        pltpu.VMEM((width, 128), BF16),
        pltpu.VMEM((nz, rows, 128), BF16),
        pltpu.VMEM((nz, rows, 128), BF16),
    ]
    for n in (12, 1, nz, 6, 7, 1, 1, 1, nz, 1, nz, 1, nz, 1, 1):
        scratch.append(pltpu.SemaphoreType.DMA((n,)))
    made = pl.pallas_call(
        functools.partial(layer_kernel, nx, ny, nz, cap),
        out_shape=jax.ShapeDtypeStruct((rows, 384), F32),
        in_specs=[hbm] * 15,
        out_specs=hbm,
        scratch_shapes=scratch,
        compiler_params=pltpu.CompilerParams(
            collective_id=0, has_side_effects=True, vmem_limit_bytes=64000000
        ),
        name="layer",
    )(
        tokens, prior_state.reshape(rows, DK, DV), decay_rate, norm_in.reshape(2 * nz, 128),
        query_weight.T, key_weight.T, value_weight, gate_weight, out_weight,
        norm_moe.reshape(2 * nz, 128), routes.T, route_weight.T,
        expert_gate.reshape(full, ffe).T, expert_up.reshape(full, ffe).T, expert_down.reshape(ffe, full),
    )
    next_hidden, new_state = pl.pallas_call(
        state_kernel,
        out_shape=(jax.ShapeDtypeStruct((rows, 128), BF16), jax.ShapeDtypeStruct((rows, DK, DV), F32)),
        in_specs=[pl.BlockSpec(memory_space=pltpu.SMEM), vmem, vmem],
        out_specs=(hbm, hbm),
        scratch_shapes=[
            pltpu.VMEM((rows, 128), BF16),
            pltpu.VMEM((rows, DK, DV), F32),
            pltpu.SemaphoreType.DMA((9,)),
        ],
        compiler_params=pltpu.CompilerParams(vmem_limit_bytes=16 * 1024 * 1024),
        name="state",
    )(decay_rate, made, prior_state.reshape(rows, DK, DV))
    return (next_hidden, new_state[:, None])


def solution(mesh):
    n_ep, n_tp = mesh.shape["ep"], mesh.shape["tp"]
    nx = next(i for i in range(1, n_ep + 1) if i * i >= n_ep)
    placed = (
        P("ep", "tp"),
        P("ep", "tp", None, None),
        P("tp"),
        P(),
        P(None, "tp"),
        P(None, "tp"),
        P(None, "tp"),
        P(None, "tp"),
        P("tp", None),
        P(),
        P(),
        P(),
        P("ep", None, "tp"),
        P("ep", None, "tp"),
        P("ep", "tp", None),
    )
    return jax.shard_map(
        functools.partial(on_device, nx, n_ep // nx, n_tp // 2),
        mesh=mesh,
        in_specs=placed,
        out_specs=(P("ep", "tp"), P("ep", "tp", None, None)),
        check_vma=False,
    )
```

time: 55.1 us -> 53.2 us (0.966)
  Pallas kernels: 53.7 us -> 50.8 us
  local copies, waits for them, and re-layouts: 0 us -> 0.89 us
    pallas_call x1, Pallas kernels: 3.08 us -> 1.53 us  [on_device(): pl.pallas_call(state_kernel, out_shape=(jax.ShapeDtypeStruct((rows, 128),...]
    pallas_call x1, Pallas kernels: 50.6 us -> 49.3 us  [on_device(): pl.pallas_call(functools.partial(layer_kernel, nx, ny, nz, cap), out_shap...]
    unnamed x0 -> x4, local copies, waits for them, and re-layouts: none -> 0.89 us
where the time goes in v4:
time: 53.2 us; the launch traced here: 53 us
  Pallas kernels  50.8 us (95%)
  between operations  1.31 us (2%)
  local copies, waits for them, and re-layouts  0.89 us (2%)
    pallas_call x1, Pallas kernels, on_device(): pl.pallas_call(functools.partial(layer_kernel, nx, ny, nz, cap), out_shap...  49.3 us
    pallas_call x1, Pallas kernels, on_device(): pl.pallas_call(state_kernel, out_shape=(jax.ShapeDtypeStruct((rows, 128),...  1.53 us

profile of v4, /device:TPU:1, one launch (start us, length us, event | category | flops | bytes accessed | tf_op | source)
XLA Modules:
  0.0 53.0 jit_solution(12730667226421692886)
XLA Ops:
  1.3 0.0 copy-start
  1.3 49.3 %layer.1.made = f32[64,384]{1,0:T(8,128)} custom-call(bf16[64,128]{1,0:T(8,128)(2,1)} %tokens.1, f32[64,64,128]{2,1,0:T(8,128)} %bitcast.17, f32[1]{0:T(128)S(6)} %copy.18.decay_in.decay, f32[16,128]{1,0:T(8,128)} %bitcast.24, bf16[64,2048]{1,0:T(8,128)(2,1)} %bitcast.22, bf16[64,2048]{1,0:T(8,128)(2,1)} %bitcast.23, bf16[2048,128]{1,0:T(8,128)(2,1)} %wv.1, ...), custom_call_target="tpu_custom_call" | custom-call | tf_op jit(solution)/shard_map/layer/pallas_call | solution.py:497
  50.6 0.0 copy-done
  50.6 0.0 copy-start.1
  50.6 0.9 %copy-done.1 = f32[64,384]{1,0:T(8,128)S(1)} copy-done((f32[64,384]{1,0:T(8,128)S(1)}, f32[64,384]{1,0:T(8,128)}, u32[]{:S(2)}) %copy-start.1) | copy-done | bytes 98328
  51.5 1.5 %state.1 = (bf16[64,128]{1,0:T(8,128)(2,1)}, f32[64,64,128]{2,1,0:T(8,128)}) custom-call(f32[1]{0:T(128)S(6)} %copy.18.decay_in.decay, f32[64,384]{1,0:T(8,128)S(1)} %copy-done.1, f32[64,64,128]{2,1,0:T(8,128)S(1)} %bitcast.18), custom_call_target="tpu_custom_call" | custom-call | tf_op jit(solution)/shard_map/state/pallas_call | solution.py:513
Async XLA Ops:
  1.3 49.3 %copy-start = (f32[64,1,64,128]{3,2,1,0:T(8,128)S(1)}, f32[64,1,64,128]{3,2,1,0:T(8,128)}, u32[]{:S(2)}) copy-start(f32[64,1,64,128]{3,2,1,0:T(8,128)} %param.16) | copy-start | bytes 6291460
  50.6 0.9 %copy-start.1 = (f32[64,384]{1,0:T(8,128)S(1)}, f32[64,384]{1,0:T(8,128)}, u32[]{:S(2)}) copy-start(f32[64,384]{1,0:T(8,128)} %layer.1.made) | copy-start | bytes 294916

commit v5 on v4

--- a/solution.py
+++ b/solution.py
@@ -30,11 +30,12 @@
     decay, tok_own, tok, wqk_v, wvg_v, prior_v, norms, rt_v, rw_v, keep2,
     halves, q_s, k_s, v_s, kv_in, k_all, wo2, ps, pr, resz, sel, x2, xg, sq, acc, wgu, wd2,
     ds, ret, flat, qs, qr,
-    ld, p1s, p1r, wds, wdr, p3s, p3r, p4s, p4r, p5s, p5r, p6s, p6r, p7s, p7r,
+    ld, p1s, p1r, wds, wdr, p3s, p3r, p4s, p5s, p5r, p6s, p7s,
 ):
     n_ep = nx * ny
     rows = tokens.shape[0]
     nin_v, nmoe_v = norms.at[0], norms.at[1]
+    p4r, p6r, p7r = p1r, p1r, p3r
     ep = lax.axis_index("ep")
     tp = lax.axis_index("tp")
     z = lax.div(tp, 2)
@@ -263,13 +264,12 @@
     mixed = jnp.concatenate(sides, 1)
     loaded(8, wo2.at[part_of(c, 128), :])
     arrived(wo2.at[part_of(o, 128), :], wdr.at[3])
-    made = jnp.dot(mixed, wo2[...], preferred_element_type=F32).astype(BF16)
-    for j in range(2 * nz):
-        ps[j] = made[:, j * 128 : (j + 1) * 128]
-
     for d in z_order[::-1] + [0]:
+        cols = pl.ds(pl.multiple_of(up_z(d) * 256, 256), 256)
+        made = jnp.dot(mixed, wo2[:, cols], preferred_element_type=F32).astype(BF16)
         for p in range(2):
             at = 2 * up_z(d) + p
+            ps[at] = made[:, p * 128 : (p + 1) * 128]
             copy = remote(ps.at[at], pr.at[c, d], p3s.at[0], p3r.at[0], ep, at)
             if d:
                 go(copy)
@@ -303,7 +303,7 @@
             for e in range(n_ep):
                 sel[e, i] = rows_out[e * SLOT : e * SLOT + cap, :]
         span = slice(cuts[g], cuts[g + 1])
-        for d in ep_order:
+        for d in ep_order[::-1]:
             e = up_ep(d)
             remote(
                 sel.at[e, span], x2.at[c, d // 2, span], p5s.at[0], p5r.at[g], e, 2 * z + d % 2
@@ -344,12 +344,12 @@
             )
             if first_join:
                 acc[...] = more
-            else:
+            elif i + 1 < nz:
                 acc[...] += more
             first_join, wide = False, []
     scale = lax.rsqrt(jnp.sum(sq[...], -1, keepdims=True) / (2 * half) + EPSILON)
-    gate_part = acc[:, : 2 * hid_rows] * scale
-    up_part = acc[:, 2 * hid_rows :] * scale
+    gate_part = (acc[:, : 2 * hid_rows] + more[:, : 2 * hid_rows]) * scale
+    up_part = (acc[:, 2 * hid_rows :] + more[:, 2 * hid_rows :]) * scale
     hidden = (gate_part * jax.nn.sigmoid(gate_part) * up_part).astype(BF16)
     loaded(10, wd2.at[mine, :])
     arrived(wd2.at[mine, :], wdr.at[6])
@@ -492,7 +492,7 @@
         pltpu.VMEM((nz, rows, 128), BF16),
         pltpu.VMEM((nz, rows, 128), BF16),
     ]
-    for n in (12, 1, nz, 6, 7, 1, 1, 1, nz, 1, nz, 1, nz, 1, 1):
+    for n in (12, 1, nz, 6, 7, 1, 1, 1, 1, nz, 1, 1):
         scratch.append(pltpu.SemaphoreType.DMA((n,)))
     made = pl.pallas_call(
         functools.partial(layer_kernel, nx, ny, nz, cap),

time: 53.2 us -> 52.7 us (level)
  no operation moved by 1% of the time
where the time goes in v5:
time: 52.7 us; the launch traced here: 52.6 us
  Pallas kernels  50.4 us (96%)
  between operations  1.31 us (2%)
  local copies, waits for them, and re-layouts  0.89 us (2%)
    pallas_call x1, Pallas kernels, on_device(): pl.pallas_call(functools.partial(layer_kernel, nx, ny, nz, cap), out_shap...  48.9 us
    pallas_call x1, Pallas kernels, on_device(): pl.pallas_call(state_kernel, out_shape=(jax.ShapeDtypeStruct((rows, 128),...  1.53 us

profile of v5, /device:TPU:1, one launch (start us, length us, event | category | flops | bytes accessed | tf_op | source)
XLA Modules:
  0.0 52.6 jit_solution(10899820614606848298)
XLA Ops:
  1.3 0.0 copy-start
  1.3 48.9 %layer.1.made = f32[64,384]{1,0:T(8,128)} custom-call(bf16[64,128]{1,0:T(8,128)(2,1)} %tokens.1, f32[64,64,128]{2,1,0:T(8,128)} %bitcast.17, f32[1]{0:T(128)S(6)} %copy.18.decay_in.decay, f32[16,128]{1,0:T(8,128)} %bitcast.24, bf16[64,2048]{1,0:T(8,128)(2,1)} %bitcast.22, bf16[64,2048]{1,0:T(8,128)(2,1)} %bitcast.23, bf16[2048,128]{1,0:T(8,128)(2,1)} %wv.1, ...), custom_call_target="tpu_custom_call" | custom-call | tf_op jit(solution)/shard_map/layer/pallas_call | solution.py:497
  50.1 0.0 copy-done
  50.2 0.0 copy-start.1
  50.2 0.9 %copy-done.1 = f32[64,384]{1,0:T(8,128)S(1)} copy-done((f32[64,384]{1,0:T(8,128)S(1)}, f32[64,384]{1,0:T(8,128)}, u32[]{:S(2)}) %copy-start.1) | copy-done | bytes 98328
  51.1 1.5 %state.1 = (bf16[64,128]{1,0:T(8,128)(2,1)}, f32[64,64,128]{2,1,0:T(8,128)}) custom-call(f32[1]{0:T(128)S(6)} %copy.18.decay_in.decay, f32[64,384]{1,0:T(8,128)S(1)} %copy-done.1, f32[64,64,128]{2,1,0:T(8,128)S(1)} %bitcast.18), custom_call_target="tpu_custom_call" | custom-call | tf_op jit(solution)/shard_map/state/pallas_call | solution.py:513
Async XLA Ops:
  1.3 48.9 %copy-start = (f32[64,1,64,128]{3,2,1,0:T(8,128)S(1)}, f32[64,1,64,128]{3,2,1,0:T(8,128)}, u32[]{:S(2)}) copy-start(f32[64,1,64,128]{3,2,1,0:T(8,128)} %param.16) | copy-start | bytes 6291460
  50.2 0.9 %copy-start.1 = (f32[64,384]{1,0:T(8,128)S(1)}, f32[64,384]{1,0:T(8,128)}, u32[]{:S(2)}) copy-start(f32[64,384]{1,0:T(8,128)} %layer.1.made) | copy-start | bytes 294916

commit v6 on v5

--- a/solution.py
+++ b/solution.py
@@ -285,6 +285,7 @@
     out[:, 256:384] = jnp.concatenate([k_all[...].T[:DK, :], jnp.zeros((DK, 128 - rows), F32)], 1)
     out[part_of(c, part), 128:256] = v_s[c]
     out[part_of(o, part), 128:256] = kv_in[1]
+    load(11, out.at[:, 128:384], out_hbm.at[:, 128:384])
     arrived(ps.at[0 : 2 * nz - 1], p3r.at[0])
     for p in range(2):
         total = tok_own[p * part : (p + 1) * part, :].astype(F32)
@@ -407,7 +408,6 @@
         total += qr[d].astype(F32)
     out[:, :128] = total.astype(BF16).astype(F32)
     load(11, out.at[:, 0:128], out_hbm.at[:, 0:128])
-    load(11, out.at[:, 128:384], out_hbm.at[:, 128:384])
     left(ps.at[0 : 2 * nz - 1], p1s.at[0])
     left(ps.at[0 : 2 * nz - 1], p3s.at[0])
     left(resz.at[1:nz], p4s.at[0])
@@ -425,21 +425,20 @@
 
 
 def state_kernel(decay, made, prior, hidden_out, state_out, hidden, state, sems):
-    pieces = 8
+    pieces = 16
     size = state.shape[0] // pieces
     hidden[...] = made[:, :128].astype(BF16)
-    stores = [pltpu.make_async_copy(hidden, hidden_out, sems.at[pieces])]
-    stores[0].start()
+    first = pltpu.make_async_copy(hidden, hidden_out, sems.at[0])
+    first.start()
     keep = 1.0 - decay[0]
     for j in range(pieces):
         for row in range(j * size, (j + 1) * size):
             key, value = made[:, 256 + row : 257 + row], made[row : row + 1, 128:256]
             state[row] = keep * prior[row] + key * value
         span = slice(j * size, (j + 1) * size)
-        stores.append(pltpu.make_async_copy(state.at[span], state_out.at[span], sems.at[j]))
-        stores[-1].start()
-    for copy in stores:
-        copy.wait()
+        pltpu.make_async_copy(state.at[span], state_out.at[span], sems.at[1]).start()
+    first.wait()
+    pltpu.make_async_copy(state, state_out, sems.at[1]).wait()
 
 
 def on_device(
@@ -518,7 +517,7 @@
         scratch_shapes=[
             pltpu.VMEM((rows, 128), BF16),
             pltpu.VMEM((rows, DK, DV), F32),
-            pltpu.SemaphoreType.DMA((9,)),
+            pltpu.SemaphoreType.DMA((2,)),
         ],
         compiler_params=pltpu.CompilerParams(vmem_limit_bytes=16 * 1024 * 1024),
         name="state",

time: 52.7 us -> 52.6 us (level)
  no operation moved by 1% of the time
where the time goes in v6:
time: 52.6 us; the launch traced here: 52.5 us
  Pallas kernels  50.2 us (95%)
  between operations  1.31 us (2%)
  local copies, waits for them, and re-layouts  0.89 us (2%)
    pallas_call x1, Pallas kernels, on_device(): pl.pallas_call(functools.partial(layer_kernel, nx, ny, nz, cap), out_shap...  48.8 us
    pallas_call x1, Pallas kernels, on_device(): pl.pallas_call(state_kernel, out_shape=(jax.ShapeDtypeStruct((rows, 128),...  1.42 us

profile of v6, /device:TPU:1, one launch (start us, length us, event | category | flops | bytes accessed | tf_op | source)
XLA Modules:
  0.0 52.5 jit_solution(13395207004757461943)
XLA Ops:
  1.3 0.0 copy-start
  1.3 48.8 %layer.1.made = f32[64,384]{1,0:T(8,128)} custom-call(bf16[64,128]{1,0:T(8,128)(2,1)} %tokens.1, f32[64,64,128]{2,1,0:T(8,128)} %bitcast.17, f32[1]{0:T(128)S(6)} %copy.18.decay_in.decay, f32[16,128]{1,0:T(8,128)} %bitcast.24, bf16[64,2048]{1,0:T(8,128)(2,1)} %bitcast.22, bf16[64,2048]{1,0:T(8,128)(2,1)} %bitcast.23, bf16[2048,128]{1,0:T(8,128)(2,1)} %wv.1, ...), custom_call_target="tpu_custom_call" | custom-call | tf_op jit(solution)/shard_map/layer/pallas_call | solution.py:496
  50.1 0.0 copy-done
  50.1 0.0 copy-start.1
  50.1 0.9 %copy-done.1 = f32[64,384]{1,0:T(8,128)S(1)} copy-done((f32[64,384]{1,0:T(8,128)S(1)}, f32[64,384]{1,0:T(8,128)}, u32[]{:S(2)}) %copy-start.1) | copy-done | bytes 98328
  51.0 1.4 %state.1 = (bf16[64,128]{1,0:T(8,128)(2,1)}, f32[64,64,128]{2,1,0:T(8,128)}) custom-call(f32[1]{0:T(128)S(6)} %copy.18.decay_in.decay, f32[64,384]{1,0:T(8,128)S(1)} %copy-done.1, f32[64,64,128]{2,1,0:T(8,128)S(1)} %bitcast.18), custom_call_target="tpu_custom_call" | custom-call | tf_op jit(solution)/shard_map/state/pallas_call | solution.py:512
Async XLA Ops:
  1.3 48.9 %copy-start = (f32[64,1,64,128]{3,2,1,0:T(8,128)S(1)}, f32[64,1,64,128]{3,2,1,0:T(8,128)}, u32[]{:S(2)}) copy-start(f32[64,1,64,128]{3,2,1,0:T(8,128)} %param.16) | copy-start | bytes 6291460
  50.1 0.9 %copy-start.1 = (f32[64,384]{1,0:T(8,128)S(1)}, f32[64,384]{1,0:T(8,128)}, u32[]{:S(2)}) copy-start(f32[64,384]{1,0:T(8,128)} %layer.1.made) | copy-start | bytes 294916
